TPU v7x, 512 devices: a whole 4x8x8 slice. The times are simulated.
512 devices in a mesh: rep: 64 (over z, y), fs: 4 (over x), tp: 2 (over core).
Axes of the slice: x: 4, y: 8, z: 8, core: 2. Of those that a mesh axis runs over, the one named last changes fastest.
Arguments:
- gate_pre: bfloat16 [40960, 2816], P(('rep', 'fs'), 'tp'), may hold values from -6 to 6
- up_pre: bfloat16 [40960, 2816], P(('rep', 'fs'), 'tp'), may hold values from -6 to 6
- gate_taps: bfloat16 [3, 2816], P(None, 'tp'), may hold values from -3 to 3
- up_taps: bfloat16 [3, 2816], P(None, 'tp'), may hold values from -3 to 3
- down_weight: bfloat16 [2816, 2048], P('tp', 'fs'), may hold values from -0.125 to 0.125
- cotangent: bfloat16 [40960, 2048], P('rep', 'fs'), may hold values from -16 to 16
Outputs:
- grad_gate: bfloat16 [40960, 2816], P(('rep', 'fs'), 'tp')
- grad_up: bfloat16 [40960, 2816], P(('rep', 'fs'), 'tp')
- grad_gate_taps: float32 [3, 2816], P(None, 'tp')
- grad_up_taps: float32 [3, 2816], P(None, 'tp')
- grad_down: float32 [4, 512, 2816], P('fs', 'rep', 'tp')
- down_norms: float32 [2816], P('tp')
All inputs are finite; a program needn't handle non-finite values.
Results may differ from a plain program's by a relative error of at most 0.0049.
Values may be sent and summed in bfloat16 or wider, within the bound.
No kernel may reach another device: no remote copies, remote signals or barrier semaphores. Data moves between devices by JAX's collectives and lax.ppermute only.
A program may use at most 64 MiB of HBM per device.

v0:
```python
import functools

import jax
import jax.numpy as jnp
from jax import lax
from jax.experimental import pallas as pl
from jax.experimental.pallas import tpu as pltpu
from jax.sharding import Mesh
from jax.sharding import PartitionSpec as P


D = 2048
ZY = ("zh", "zl", "yh", "yl")
TOK = ("zh", "zl", "yh", "yl", "fs")
NEAR = ("zl", "yl", "fs")
FAR = ("zh", "yh")
HALO = 2
PAD = 8
LANE = 128
GROUP = 4
F32 = jnp.float32
BF16 = jnp.bfloat16


def passed_along(array, axis, by):
    count = lax.axis_size(axis)
    pairs = [(i, i + by) for i in range(count) if 0 <= i + by < count]
    return lax.ppermute(array, axis, pairs)


def swap(array, axes):
    return lax.all_to_all(array, axes, 0, 0, tiled=True)


def call(body, out_shape, flops=0, limit=8, **kw):
    return pl.pallas_call(
        body,
        out_shape=out_shape,
        compiler_params=pltpu.CompilerParams(vmem_limit_bytes=limit << 20),
        cost_estimate=pl.CostEstimate(flops=flops, bytes_accessed=1 << 20, transcendentals=0),
        **kw,
    )


def hidden_body(rows, width, gate_ref, up_ref, before_ref, gate_taps, up_taps, out_ref, held_ref):
    step = pl.program_id(0)
    block = gate_ref.shape[1]

    def conv(which, source, taps):
        held_ref[PAD - HALO : PAD] = before_ref[which].astype(F32)
        held_ref[PAD : PAD + rows] = source[...].astype(F32)
        total = taps[2:3].astype(F32) * held_ref[PAD : PAD + rows]
        for k in range(2):
            start = PAD - HALO + k
            total += taps[k : k + 1].astype(F32) * held_ref[start : start + rows]
        return total

    gate = conv(0, gate_ref, gate_taps)
    up = conv(1, up_ref, up_taps)
    value = gate * (1.0 / (1.0 + jnp.exp(-gate))) * up
    lane = lax.broadcasted_iota(jnp.int32, value.shape, 1) + step * block
    value = jnp.where(lane < width, value, 0.0).astype(BF16)
    for k in range(out_ref.shape[1]):
        out_ref[0, k] = value


def hidden_of(gate_pre, up_pre, before, gate_taps, up_taps, block, n_fs):
    rows, width = gate_pre.shape
    wide = pl.BlockSpec((rows, block), lambda i: (0, i))
    taps = pl.BlockSpec((3, block), lambda i: (0, i))
    return call(
        functools.partial(hidden_body, rows, width),
        jax.ShapeDtypeStruct((GROUP, n_fs, rows, block), BF16),
        flops=40 * rows * width,
        limit=60,
        grid=(GROUP,),
        in_specs=[wide, wide, pl.BlockSpec((2, HALO, block), lambda i: (0, 0, i)), taps, taps],
        out_specs=pl.BlockSpec((1, n_fs, rows, block), lambda i: (i, 0, 0, 0)),
        scratch_shapes=[pltpu.VMEM((rows + PAD, block), F32)],
    )(gate_pre, up_pre, before, gate_taps, up_taps)


def terms_body(rows, at_ref, cot_ref, weight_ref, *refs):
    *outs, held_ref = refs
    tokens = cot_ref.shape[0]
    held_ref[:tokens] = cot_ref[...]
    held_ref[tokens:] = jnp.zeros((held_ref.shape[0] - tokens, held_ref.shape[1]), BF16)
    for k, out in enumerate(outs):
        start = pl.multiple_of(at_ref[k] * rows, 16)
        out[...] = lax.dot_general(
            held_ref[pl.ds(start, rows + PAD)],
            weight_ref[...],
            (((1,), (1,)), ((), ())),
            preferred_element_type=F32,
        ).astype(BF16)


def terms_of(at, cotangent, weight, rows):
    tokens, depth = cotangent.shape
    width = weight.shape[0]
    whole = pl.BlockSpec(memory_space=pltpu.VMEM)
    steps = tokens // rows
    return call(
        functools.partial(terms_body, rows),
        (jax.ShapeDtypeStruct((rows + PAD, width), BF16),) * steps,
        flops=2 * tokens * depth * width,
        limit=16,
        in_specs=[pl.BlockSpec(memory_space=pltpu.SMEM), whole, whole],
        out_specs=(whole,) * steps,
        scratch_shapes=[pltpu.VMEM((tokens + 2 * PAD, depth), BF16)],
    )(at, cotangent, weight)


def grad_body(order_ref, own_ref, side_ref, far_ref, across_ref, hidden_ref, out_ref, total_ref):
    step = pl.program_id(0)
    for k, ref in enumerate((own_ref, side_ref, far_ref)):

        @pl.when(step == k)
        def _(ref=ref, k=k):
            part = lax.dot_general(
                ref[...], hidden_ref[0], (((0,), (0,)), ((), ())), preferred_element_type=F32
            )
            total_ref[...] = part if k == 0 else total_ref[...] + part

    @pl.when(step >= 3)
    def _():
        part = lax.dot_general(
            across_ref[0], hidden_ref[0], (((0,), (0,)), ((), ())), preferred_element_type=F32
        )
        total_ref[...] += part

    @pl.when(step == pl.num_programs(0) - 1)
    def _():
        out_ref[...] = total_ref[...].astype(BF16).reshape(out_ref.shape)


def grad_of(order, own, side, far, across, hidden, n_rep):
    tokens, depth = own.shape
    block = hidden.shape[2]
    shape = (n_rep, depth // n_rep, block)
    same = pl.BlockSpec((tokens, depth), lambda i, order: (0, 0))
    return call(
        grad_body,
        jax.ShapeDtypeStruct(shape, BF16),
        flops=2 * GROUP * tokens * depth * block,
        limit=60,
        grid_spec=pltpu.PrefetchScalarGridSpec(
            num_scalar_prefetch=1,
            grid=(GROUP + 1,),
            in_specs=[same] * 3
            + [
                pl.BlockSpec(
                    (1, tokens, depth), lambda i, order: (jnp.maximum(i - 3, 0), 0, 0)
                ),
                pl.BlockSpec((1, tokens, block), lambda i, order: (order[i], 0, 0)),
            ],
            out_specs=pl.BlockSpec(shape, lambda i, order: (0, 0, 0)),
            scratch_shapes=[pltpu.VMEM((depth, block), F32)],
        ),
    )(order, own, side, far, across, hidden)


def share_body(scale, parts_ref, taps_ref, grad_ref, small_ref):
    block = parts_ref.shape[2]
    copies, rows, width = small_ref.shape
    for zl in range(2):
        for yl in range(2):
            total = None
            for zh in range(4):
                for yh in range(4):
                    part = parts_ref[((zh * 2 + zl) * 4 + yh) * 2 + yl].astype(F32)
                    total = part if total is None else total + part
            start = (zl * 2 + yl) * block
            size = min(block, width - start)
            grad_ref[:, start : start + size] = total[:, :size] * scale
    value = grad_ref[...]
    norm = jnp.sum(value * value, axis=0, keepdims=True)
    row = lax.broadcasted_iota(jnp.int32, (rows, width), 0)
    small = jnp.where(row == rows - 1, norm, taps_ref[...]).astype(BF16)
    for k in range(copies):
        small_ref[k] = small


def chain_body(rows, *refs):
    *terms, gate_ref, up_ref, before_ref, after_ref, gate_taps, up_taps = refs[:10]
    gate_out, up_out, taps_out, gate_held, up_held, gate_back, up_back = refs[10:]
    reach = terms[0].shape[0]
    for at in range(0, gate_ref.shape[1], LANE):
        lanes = slice(at, at + LANE)

        def conv(which, source, taps, held):
            held[PAD - HALO : PAD] = before_ref[which, :, lanes].astype(F32)
            held[PAD : PAD + rows] = source[:, lanes].astype(F32)
            held[PAD + rows : PAD + rows + HALO] = after_ref[which, :, lanes].astype(F32)
            coef = [taps[k : k + 1, lanes].astype(F32) for k in range(3)]
            total = coef[2] * held[PAD : PAD + reach]
            for k in range(2):
                total += coef[k] * held[PAD - HALO + k : PAD - HALO + k + reach]
            return total, coef

        gate, gate_coef = conv(0, gate_ref, gate_taps, gate_held)
        up, up_coef = conv(1, up_ref, up_taps, up_held)
        d_hidden = terms[0][:, lanes].astype(F32)
        for term in terms[1:]:
            d_hidden += term[:, lanes].astype(F32)
        sig = 1.0 / (1.0 + jnp.exp(-gate))
        gate_back[...] = d_hidden * up * sig * (1.0 + gate * (1.0 - sig))
        up_back[...] = d_hidden * gate * sig

        def back(coef, held, out):
            total = coef[2] * held[:rows]
            for k in range(2):
                total += coef[k] * held[2 - k : 2 - k + rows]
            out[:, lanes] = total.astype(BF16)

        back(gate_coef, gate_back, gate_out)
        back(up_coef, up_back, up_out)
        for first, held, source in ((0, gate_back, gate_held), (3, up_back, up_held)):
            for k in range(3):
                start = PAD - HALO + k
                product = held[:rows] * source[start : start + rows]
                taps_out[first + k : first + k + 1, lanes] = jnp.sum(product, 0, keepdims=True)
        taps_out[6:, lanes] = jnp.zeros((2, LANE), F32)


def chain_of(terms, gate_pre, up_pre, before, after, gate_taps, up_taps, block):
    rows, width = gate_pre.shape
    reach = terms[0].shape[0]
    tall = pl.BlockSpec((reach, block), lambda i: (0, i))
    wide = pl.BlockSpec((rows, block), lambda i: (0, i))
    edge = pl.BlockSpec((2, HALO, block), lambda i: (0, 0, i))
    taps = pl.BlockSpec((3, block), lambda i: (0, i))
    grad = jax.ShapeDtypeStruct((rows, width), BF16)
    return call(
        functools.partial(chain_body, rows),
        (grad, grad, jax.ShapeDtypeStruct((8, width), F32)),
        flops=100 * rows * width,
        limit=60,
        grid=(GROUP,),
        in_specs=[tall] * 4 + [wide, wide, edge, edge, taps, taps],
        out_specs=(wide, wide, pl.BlockSpec((8, block), lambda i: (0, i))),
        scratch_shapes=[pltpu.VMEM((reach + PAD, LANE), F32)] * 2
        + [pltpu.VMEM((reach, LANE), F32)] * 2,
    )(*terms, gate_pre, up_pre, before, after, gate_taps, up_taps)


def total_of(seen_ref):
    total = None
    for source in range(seen_ref.shape[0]):
        part = seen_ref[source].astype(F32)
        total = part if total is None else total + part
    return total


def middle_body(seen_ref, small_ref):
    total = total_of(seen_ref).astype(BF16)
    for k in range(small_ref.shape[0]):
        small_ref[k] = total


def last_body(scale, seen_ref, gate_ref, up_ref, norm_ref):
    total = total_of(seen_ref)
    gate_ref[...] = total[:3] * scale
    up_ref[...] = total[3:6] * scale
    norm_ref[...] = total[7:] / D


def local(gate_pre, up_pre, gate_taps, up_taps, down_weight, cotangent):
    rows, width = gate_pre.shape
    n_fs = lax.axis_size("fs")
    n_rep = lax.axis_size(ZY)
    n_near = lax.axis_size(NEAR)
    n_far = lax.axis_size(FAR)
    block = -(-(width // LANE) // GROUP) * LANE
    grad_scale = float(rows * n_rep * n_fs) ** (-0.5)

    before = passed_along(jnp.stack([gate_pre[-HALO:], up_pre[-HALO:]]), "fs", 1)
    after = passed_along(jnp.stack([gate_pre[:HALO], up_pre[:HALO]]), "fs", -1)

    axes = ("zl", "yl", "tp")
    first, second = [], []
    for i in range(8):
        flip = 4 if i % 2 == 0 else 2
        first.append((i, i ^ flip))
        if i % 2 == 0:
            second.append((i, i ^ 6))
    side = lax.ppermute(cotangent, axes, first)
    far = lax.ppermute(cotangent, axes, second)
    across = lax.ppermute(jnp.stack([side, far]), "tp", [(0, 1), (1, 0)])
    tp = lax.axis_index("tp")
    member = lax.axis_index("zl") * 2 + lax.axis_index("yl")
    order = jnp.stack(
        [member, member ^ (2 - tp), member ^ 3, member ^ (1 + tp), member ^ 3]
    )

    hidden = hidden_of(gate_pre, up_pre, before, gate_taps, up_taps, block, n_fs)
    everyone = swap(hidden.reshape(n_near, rows, block), NEAR)

    me = lax.axis_index("fs")
    steps = (1, 3, 2, 0)
    hidden, cot_late = lax.optimization_barrier((hidden, cotangent))
    at = jnp.stack([(me + step) % n_fs for step in steps])
    terms = list(terms_of(at, cot_late, down_weight, rows))
    for k, step in enumerate(steps[:3]):
        pairs = [(i, (i + step) % n_fs) for i in range(n_fs)]
        terms[k] = lax.ppermute(terms[k], "fs", pairs)

    partial = grad_of(
        order, cotangent, side, far, across, everyone.reshape(GROUP, -1, block), n_rep
    )
    parts = swap(partial, ZY)

    grad_gate, grad_up, taps = chain_of(
        terms, gate_pre, up_pre, before, after, gate_taps, up_taps, block
    )

    wide = jax.ShapeDtypeStruct((8, width), F32)
    sent = functools.partial(jax.ShapeDtypeStruct, dtype=BF16)
    grad_share, small = call(
        functools.partial(share_body, grad_scale), (wide, sent((n_near, 8, width)))
    )(parts, taps)
    small = call(middle_body, sent((n_far, 8, width)))(swap(small, NEAR))
    three = jax.ShapeDtypeStruct((3, width), F32)
    gate_out, up_out, norms = call(
        functools.partial(last_body, grad_scale),
        (three, three, jax.ShapeDtypeStruct((1, width), F32)),
    )(swap(small, FAR))
    return grad_gate, grad_up, gate_out, up_out, grad_share[None], norms[0]


def solution(mesh):
    finer = Mesh(
        mesh.devices.reshape(4, 2, 4, 2, mesh.shape["fs"], mesh.shape["tp"]),
        ("zh", "zl", "yh", "yl", "fs", "tp"),
    )
    in_specs = (P(TOK, "tp"), P(TOK, "tp"), P(None, "tp"), P(None, "tp"), P("tp", "fs"), P(ZY, "fs"))
    out_specs = (P(TOK, "tp"), P(TOK, "tp"), P(None, "tp"), P(None, "tp"), P("fs", ZY, "tp"), P("tp"))
    return jax.shard_map(local, mesh=finer, in_specs=in_specs, out_specs=out_specs, check_vma=False)
```

profile of v0, /device:TPU:16, one launch (start us, length us, event | category | flops | bytes accessed | tf_op | source)
XLA Modules:
  0.0 164.8 jit_solution(958822677842721621)
XLA Ops:
  0.6 0.8 slice_bitcast_fusion
  1.5 3.4 %collective-permute-start = (bf16[2,2,1408]{2,1,0:T(2,128)(2,1)S(1)}, bf16[2,2,1408]{2,1,0:T(2,128)(2,1)S(1)}, u32[]{:S(2)}, u32[]{:S(2)}) collective-permute-start(bf16[2,2,1408]{2,1,0:T(2,128)(2,1)S(1)} %pad_maximum_fusion.1), channel_id=1, source_target_pairs={{0,2},{2,4},{4,6},{1,3},{3,5},{5,7},{8,10},{10,12},{12,14},{9,11},... | collective-permute-start | bytes 33800 | tf_op jit(solution)/shard_map/ppermute | solution.py:28
  4.9 1.4 collective-permute-done.before_ref.refs_6_
  6.3 0.6 copy-done.11
  6.9 4.2 %shard_map.109 = bf16[4,4,160,384]{3,2,1,0:T(8,128)(2,1)} custom-call(bf16[160,1408]{1,0:T(8,128)(2,1)} %refs_4_.1, bf16[160,1408]{1,0:T(8,128)(2,1)} %refs_5_.1, bf16[2,2,1408]{2,1,0:T(2,128)(2,1)} %copy-done.11, bf16[3,1408]{1,0:T(4,128)(2,1)} %refs_8_.1, bf16[3,1408]{1,0:T(4,128)(2,1)} %refs_9_.1), custom_call_target="tpu_custom_call" | custom-call | flops 9011200 | bytes 1048576 | tf_op jit(solution)/shard_map/pallas_call | solution.py:71
  11.1 8.2 %all-to-all-start = ((bf16[16,160,384]{2,1,0:T(8,128)(2,1)}), bf16[16,160,384]{2,1,0:T(8,128)(2,1)S(1)}, u32[]{:S(2)}, u32[]{:S(2)}) async-start(bf16[16,160,384]{2,1,0:T(8,128)(2,1)} %bitcast.22), calls=%async_computation | async-start | bytes 3932160 | tf_op jit(solution)/shard_map/all_to_all | solution.py:32
  19.3 3.8 %collective-permute-start.5 = (bf16[640,512]{1,0:T(8,128)(2,1)S(1)}, bf16[640,512]{1,0:T(8,128)(2,1)S(1)}, u32[]{:S(2)}, u32[]{:S(2)}) collective-permute-start(bf16[640,512]{1,0:T(8,128)(2,1)S(1)} %copy-done), channel_id=1, source_target_pairs={{0,64},{1,9},{8,72},{9,1},{64,0},{65,73},{72,8},{73,65},{2,66},{3,... | collective-permute-start | bytes 1966088 | tf_op jit(solution)/shard_map/ppermute | solution.py:287
  23.1 3.4 %collective-permute-start.6 = (bf16[640,512]{1,0:T(8,128)(2,1)S(1)}, bf16[640,512]{1,0:T(8,128)(2,1)S(1)}, u32[]{:S(2)}, u32[]{:S(2)}) collective-permute-start(bf16[640,512]{1,0:T(8,128)(2,1)S(1)} %copy-done), channel_id=1, source_target_pairs={{0,72},{8,64},{64,8},{72,0},{2,74},{10,66},{66,10},{74,2},{4,76},{... | collective-permute-start | bytes 1966088 | tf_op jit(solution)/shard_map/ppermute | solution.py:288
  26.5 28.7 %collective-permute-done.5.side_ref = bf16[640,512]{1,0:T(8,128)(2,1)S(1)} collective-permute-done((bf16[640,512]{1,0:T(8,128)(2,1)S(1)}, bf16[640,512]{1,0:T(8,128)(2,1)S(1)}, u32[]{:S(2)}, u32[]{:S(2)}) %collective-permute-start.5) | collective-permute-done | bytes 655392 | tf_op jit(solution)/shard_map/ppermute | solution.py:287
  55.2 1.3 collective-permute-done.6.far_ref
  56.5 1.3 pad_maximum_fusion
  57.8 1.9 %collective-permute-start.7 = (bf16[2,640,512]{2,1,0:T(8,128)(2,1)}, bf16[2,640,512]{2,1,0:T(8,128)(2,1)}, u32[]{:S(2)}, u32[]{:S(2)}) collective-permute-start(bf16[2,640,512]{2,1,0:T(8,128)(2,1)} %pad_maximum_fusion), channel_id=1, source_target_pairs={{0,1},{1,0},{2,3},{3,2},{4,5},{5,4},{6,7},{7,6},{8,9},{9,8},{10,11... | collective-permute-start | bytes 3932168 | tf_op jit(solution)/shard_map/ppermute | solution.py:289
  59.7 0.6 stack.73.order_ref
  60.3 2.7 %collective-permute-done.7.across_ref = bf16[2,640,512]{2,1,0:T(8,128)(2,1)} collective-permute-done((bf16[2,640,512]{2,1,0:T(8,128)(2,1)}, bf16[2,640,512]{2,1,0:T(8,128)(2,1)}, u32[]{:S(2)}, u32[]{:S(2)}) %collective-permute-start.7) | collective-permute-done | bytes 1310752 | tf_op jit(solution)/shard_map/ppermute | solution.py:289
  63.0 1.3 copy-done.5
  64.4 7.5 %shard_map.112 = bf16[64,8,384]{2,1,0:T(8,128)(2,1)} custom-call(s32[5]{0:T(128)} %stack.73.order_ref, bf16[640,512]{1,0:T(8,128)(2,1)} %own_ref.1, bf16[640,512]{1,0:T(8,128)(2,1)} %copy-done.6, bf16[640,512]{1,0:T(8,128)(2,1)} %copy-done.7, bf16[2,640,512]{2,1,0:T(8,128)(2,1)} %collective-permute-done.7.across_ref, bf16[4,640,384]{2,1,0:T(8,128)(2,1)} %bitcast.21), custom_call_target="tpu_custom_call" | custom-call | flops 1006632960 | bytes 1048576 | tf_op jit(solution)/shard_map/pallas_call | solution.py:142
  71.9 14.7 %all-to-all-start.1 = ((bf16[64,8,384]{2,1,0:T(8,128)(2,1)}), bf16[64,8,384]{2,1,0:T(8,128)(2,1)S(1)}, u32[]{:S(2)}, u32[]{:S(2)}) async-start(bf16[64,8,384]{2,1,0:T(8,128)(2,1)} %shard_map.112), calls=%async_computation.1 | async-start | bytes 786432 | tf_op jit(solution)/shard_map/all_to_all | solution.py:32
  86.7 2.4 %shard_map.110 = (bf16[168,1408]{1,0:T(8,128)(2,1)S(1)}, bf16[168,1408]{1,0:T(8,128)(2,1)S(1)}, bf16[168,1408]{1,0:T(8,128)(2,1)S(1)}, bf16[168,1408]{1,0:T(8,128)(2,1)S(1)}) custom-call(s32[4]{0:T(128)S(1)} %pad_add_fusion.at_ref, bf16[640,512]{1,0:T(8,128)(2,1)S(1)} %copy-done.1, bf16[1408,512]{1,0:T(8,128)(2,1)S(1)} %copy-done.4), custom_call_target="tpu_custom_call" | custom-call | flops 922746880 | bytes 1048576 | tf_op jit(solution)/shard_map/pallas_call | solution.py:103
  89.2 0.8 copy-done.2
  90.0 3.7 %collective-permute-start.1 = (bf16[168,1408]{1,0:T(8,128)(2,1)S(1)}, bf16[168,1408]{1,0:T(8,128)(2,1)S(1)}, u32[]{:S(2)}, u32[]{:S(2)}) collective-permute-start(bf16[168,1408]{1,0:T(8,128)(2,1)S(1)} %get-tuple-element.20), channel_id=1, source_target_pairs={{0,2},{2,4},{4,6},{6,0},{1,3},{3,5},{5,7},{7,1},{8,10},{10,12},{12... | collective-permute-start | bytes 1419272 | tf_op jit(solution)/shard_map/ppermute | solution.py:306
  93.7 3.3 %collective-permute-start.2 = (bf16[168,1408]{1,0:T(8,128)(2,1)S(1)}, bf16[168,1408]{1,0:T(8,128)(2,1)S(1)}, u32[]{:S(2)}, u32[]{:S(2)}) collective-permute-start(bf16[168,1408]{1,0:T(8,128)(2,1)S(1)} %get-tuple-element.21), channel_id=1, source_target_pairs={{0,6},{2,0},{4,2},{6,4},{1,7},{3,1},{5,3},{7,5},{8,14},{10,8},{12,... | collective-permute-start | bytes 1419272 | tf_op jit(solution)/shard_map/ppermute | solution.py:306
  97.0 3.6 %collective-permute-start.3 = (bf16[168,1408]{1,0:T(8,128)(2,1)S(1)}, bf16[168,1408]{1,0:T(8,128)(2,1)S(1)}, u32[]{:S(2)}, u32[]{:S(2)}) collective-permute-start(bf16[168,1408]{1,0:T(8,128)(2,1)S(1)} %get-tuple-element.22), channel_id=1, source_target_pairs={{0,4},{2,6},{4,0},{6,2},{1,5},{3,7},{5,1},{7,3},{8,12},{10,14},{12... | collective-permute-start | bytes 1419272 | tf_op jit(solution)/shard_map/ppermute | solution.py:306
  100.7 1.3 collective-permute-start.4
  102.0 16.0 %collective-permute-done.4.refs_7_ = bf16[2,2,1408]{2,1,0:T(2,128)(2,1)S(1)} collective-permute-done((bf16[2,2,1408]{2,1,0:T(2,128)(2,1)S(1)}, bf16[2,2,1408]{2,1,0:T(2,128)(2,1)S(1)}, u32[]{:S(2)}, u32[]{:S(2)}) %collective-permute-start.4) | collective-permute-done | bytes 11296 | tf_op jit(solution)/shard_map/ppermute | solution.py:28
  118.1 0.6 copy-done.12
  119.1 5.1 %shard_map.111 = (bf16[160,1408]{1,0:T(8,128)(2,1)}, bf16[160,1408]{1,0:T(8,128)(2,1)}, f32[8,1408]{1,0:T(8,128)}) custom-call(bf16[168,1408]{1,0:T(8,128)(2,1)} %copy-done.8, bf16[168,1408]{1,0:T(8,128)(2,1)} %copy-done.9, bf16[168,1408]{1,0:T(8,128)(2,1)} %copy-done.10, bf16[168,1408]{1,0:T(8,128)(2,1)} %copy-done.2, bf16[160,1408]{1,0:T(8,128)(2,1)} %refs_4_.1, ...), custom_call_target="tpu_custom_call" | custom-call | flops 22528000 | bytes 1048576 | tf_op jit(solution)/shard_map/pallas_call | solution.py:234
  124.3 0.8 copy-done.3
  125.1 0.7 shard_map.113
  125.7 14.2 %all_to_all.20.seen_ref = bf16[16,8,1408]{2,1,0:T(8,128)(2,1)S(1)} all-to-all(bf16[16,8,1408]{2,1,0:T(8,128)(2,1)S(1)} %get-tuple-element.27), channel_id=1, replica_groups=mesh['zh'=4,'zl'=2,'yh'=4,'yl'=2,'fs'=4,'tp'=2] {'zl','yl','fs'}, dimensions={0} | all-to-all | bytes 720896 | tf_op jit(solution)/shard_map/all_to_all | solution.py:32
  140.0 23.6 %all_to_all.21.seen_ref = bf16[16,8,1408]{2,1,0:T(8,128)(2,1)S(1)} all-to-all(bf16[16,8,1408]{2,1,0:T(8,128)(2,1)S(1)} %shard_map.114), channel_id=1, replica_groups=mesh['zh'=4,'zl'=2,'yh'=4,'yl'=2,'fs'=4,'tp'=2] {'zh','yh'}, dimensions={0} | all-to-all | bytes 720896 | tf_op jit(solution)/shard_map/all_to_all | solution.py:32
  163.5 0.7 shard_map.115
  164.2 0.6 reduce
  (30 shorter events, 0.7 us)
Async XLA Ops:
  1.5 4.8 %collective-permute-start = (bf16[2,2,1408]{2,1,0:T(2,128)(2,1)S(1)}, bf16[2,2,1408]{2,1,0:T(2,128)(2,1)S(1)}, u32[]{:S(2)}, u32[]{:S(2)}) collective-permute-start(bf16[2,2,1408]{2,1,0:T(2,128)(2,1)S(1)} %pad_maximum_fusion.1), channel_id=1, source_target_pairs={{0,2},{2,4},{4,6},{1,3},{3,5},{5,7},{8,10},{10,12},{12,14},{9,11},... | collective-permute-start | bytes 33800 | tf_op jit(solution)/shard_map/ppermute | solution.py:28
  6.3 0.6 copy-start.11
  11.1 8.2 %copy-start = (bf16[640,512]{1,0:T(8,128)(2,1)S(1)}, bf16[640,512]{1,0:T(8,128)(2,1)}, u32[]{:S(2)}) copy-start(bf16[640,512]{1,0:T(8,128)(2,1)} %own_ref.1) | copy-start | bytes 1966084
  11.1 51.9 %all-to-all-start = ((bf16[16,160,384]{2,1,0:T(8,128)(2,1)}), bf16[16,160,384]{2,1,0:T(8,128)(2,1)S(1)}, u32[]{:S(2)}, u32[]{:S(2)}) async-start(bf16[16,160,384]{2,1,0:T(8,128)(2,1)} %bitcast.22), calls=%async_computation | async-start | bytes 3932160 | tf_op jit(solution)/shard_map/all_to_all | solution.py:32
  19.3 35.9 %collective-permute-start.5 = (bf16[640,512]{1,0:T(8,128)(2,1)S(1)}, bf16[640,512]{1,0:T(8,128)(2,1)S(1)}, u32[]{:S(2)}, u32[]{:S(2)}) collective-permute-start(bf16[640,512]{1,0:T(8,128)(2,1)S(1)} %copy-done), channel_id=1, source_target_pairs={{0,64},{1,9},{8,72},{9,1},{64,0},{65,73},{72,8},{73,65},{2,66},{3,... | collective-permute-start | bytes 1966088 | tf_op jit(solution)/shard_map/ppermute | solution.py:287
  23.1 33.4 %collective-permute-start.6 = (bf16[640,512]{1,0:T(8,128)(2,1)S(1)}, bf16[640,512]{1,0:T(8,128)(2,1)S(1)}, u32[]{:S(2)}, u32[]{:S(2)}) collective-permute-start(bf16[640,512]{1,0:T(8,128)(2,1)S(1)} %copy-done), channel_id=1, source_target_pairs={{0,72},{8,64},{64,8},{72,0},{2,74},{10,66},{66,10},{74,2},{4,76},{... | collective-permute-start | bytes 1966088 | tf_op jit(solution)/shard_map/ppermute | solution.py:288
  55.2 2.6 %copy-start.6 = (bf16[640,512]{1,0:T(8,128)(2,1)}, bf16[640,512]{1,0:T(8,128)(2,1)S(1)}, u32[]{:S(2)}) copy-start(bf16[640,512]{1,0:T(8,128)(2,1)S(1)} %collective-permute-done.5.side_ref) | copy-start | bytes 1966084
  56.5 1.3 copy-start.7
  57.8 5.3 %collective-permute-start.7 = (bf16[2,640,512]{2,1,0:T(8,128)(2,1)}, bf16[2,640,512]{2,1,0:T(8,128)(2,1)}, u32[]{:S(2)}, u32[]{:S(2)}) collective-permute-start(bf16[2,640,512]{2,1,0:T(8,128)(2,1)} %pad_maximum_fusion), channel_id=1, source_target_pairs={{0,1},{1,0},{2,3},{3,2},{4,5},{5,4},{6,7},{7,6},{8,9},{9,8},{10,11... | collective-permute-start | bytes 3932168 | tf_op jit(solution)/shard_map/ppermute | solution.py:289
  63.0 1.3 copy-start.5
  64.4 22.4 %copy-start.1 = (bf16[640,512]{1,0:T(8,128)(2,1)S(1)}, bf16[640,512]{1,0:T(8,128)(2,1)}, u32[]{:S(2)}) copy-start(bf16[640,512]{1,0:T(8,128)(2,1)} %own_ref.1) | copy-start | bytes 1966084
  64.4 22.4 %copy-start.4 = (bf16[1408,512]{1,0:T(8,128)(2,1)S(1)}, bf16[1408,512]{1,0:T(8,128)(2,1)}, u32[]{:S(2)}) copy-start(bf16[1408,512]{1,0:T(8,128)(2,1)} %weight_ref.1) | copy-start | bytes 4325380
  71.9 52.4 %all-to-all-start.1 = ((bf16[64,8,384]{2,1,0:T(8,128)(2,1)}), bf16[64,8,384]{2,1,0:T(8,128)(2,1)S(1)}, u32[]{:S(2)}, u32[]{:S(2)}) async-start(bf16[64,8,384]{2,1,0:T(8,128)(2,1)} %shard_map.112), calls=%async_computation.1 | async-start | bytes 786432 | tf_op jit(solution)/shard_map/all_to_all | solution.py:32
  89.2 0.8 copy-start.2
  90.0 28.1 %collective-permute-start.1 = (bf16[168,1408]{1,0:T(8,128)(2,1)S(1)}, bf16[168,1408]{1,0:T(8,128)(2,1)S(1)}, u32[]{:S(2)}, u32[]{:S(2)}) collective-permute-start(bf16[168,1408]{1,0:T(8,128)(2,1)S(1)} %get-tuple-element.20), channel_id=1, source_target_pairs={{0,2},{2,4},{4,6},{6,0},{1,3},{3,5},{5,7},{7,1},{8,10},{10,12},{12... | collective-permute-start | bytes 1419272 | tf_op jit(solution)/shard_map/ppermute | solution.py:306
  93.7 24.3 %collective-permute-start.2 = (bf16[168,1408]{1,0:T(8,128)(2,1)S(1)}, bf16[168,1408]{1,0:T(8,128)(2,1)S(1)}, u32[]{:S(2)}, u32[]{:S(2)}) collective-permute-start(bf16[168,1408]{1,0:T(8,128)(2,1)S(1)} %get-tuple-element.21), channel_id=1, source_target_pairs={{0,6},{2,0},{4,2},{6,4},{1,7},{3,1},{5,3},{7,5},{8,14},{10,8},{12,... | collective-permute-start | bytes 1419272 | tf_op jit(solution)/shard_map/ppermute | solution.py:306
  97.0 21.0 %collective-permute-start.3 = (bf16[168,1408]{1,0:T(8,128)(2,1)S(1)}, bf16[168,1408]{1,0:T(8,128)(2,1)S(1)}, u32[]{:S(2)}, u32[]{:S(2)}) collective-permute-start(bf16[168,1408]{1,0:T(8,128)(2,1)S(1)} %get-tuple-element.22), channel_id=1, source_target_pairs={{0,4},{2,6},{4,0},{6,2},{1,5},{3,7},{5,1},{7,3},{8,12},{10,14},{12... | collective-permute-start | bytes 1419272 | tf_op jit(solution)/shard_map/ppermute | solution.py:306
  100.7 17.3 %collective-permute-start.4 = (bf16[2,2,1408]{2,1,0:T(2,128)(2,1)S(1)}, bf16[2,2,1408]{2,1,0:T(2,128)(2,1)S(1)}, u32[]{:S(2)}, u32[]{:S(2)}) collective-permute-start(bf16[2,2,1408]{2,1,0:T(2,128)(2,1)S(1)} %pad_maximum_fusion.2), channel_id=1, source_target_pairs={{2,0},{4,2},{6,4},{3,1},{5,3},{7,5},{10,8},{12,10},{14,12},{11,9},... | collective-permute-start | bytes 33800 | tf_op jit(solution)/shard_map/ppermute | solution.py:28
  118.0 0.6 copy-start.12
  118.0 0.8 copy-start.8
  118.0 0.9 copy-start.9
  118.0 1.1 copy-start.10
  124.3 0.8 copy-start.3
where the time goes:
time: 166 us; the launch traced here: 165 us
  waiting for transfers between devices  50.1 us (30%)
  starting transfers between devices  47.4 us (29%)
  blocking collectives  37.7 us (23%)
  Pallas kernels  20.7 us (12%)
  local copies, waits for them, and re-layouts  5.98 us (4%)
  other arithmetic  2 us (1%)
    all_to_all x2, blocking collectives, swap(): return lax.all_to_all(array, axes, 0, 0, tiled=True)  37.7 us
    ppermute x1, waiting for transfers between devices, local(): side = lax.ppermute(cotangent, axes, first)  28.7 us
    all_to_all x2, starting transfers between devices, swap(): return lax.all_to_all(array, axes, 0, 0, tiled=True)  22.9 us
    ppermute x2, waiting for transfers between devices, passed_along(): return lax.ppermute(array, axis, pairs)  17.4 us
    ppermute x3, starting transfers between devices, local(): terms[k] = lax.ppermute(terms[k], 'fs', pairs)  10.7 us
    pallas_call x1, Pallas kernels, grad_of(): call(grad_body, jax.ShapeDtypeStruct(shape, BF16), flops=2 * GROUP * toke...  7.55 us
    pallas_call x1, Pallas kernels, chain_of(): call(functools.partial(chain_body, rows), (grad, grad, jax.ShapeDtypeStru...  5.13 us
    ppermute x2, starting transfers between devices, passed_along(): return lax.ppermute(array, axis, pairs)  4.69 us
  transfers between devices with their start and end apart: 10, of which 5 were waited for; matrix products, arithmetic and copies ran while one was open for 1% of the time, Pallas kernels for 5%

commit v1 on v0

--- a/solution.py
+++ b/solution.py
@@ -111,58 +111,68 @@
     )(at, cotangent, weight)
 
 
-def grad_body(order_ref, own_ref, side_ref, far_ref, across_ref, hidden_ref, out_ref, total_ref):
-    step = pl.program_id(0)
-    for k, ref in enumerate((own_ref, side_ref, far_ref)):
-
-        @pl.when(step == k)
-        def _(ref=ref, k=k):
-            part = lax.dot_general(
-                ref[...], hidden_ref[0], (((0,), (0,)), ((), ())), preferred_element_type=F32
-            )
-            total_ref[...] = part if k == 0 else total_ref[...] + part
-
-    @pl.when(step >= 3)
+def grad_body(order_ref, own, side, far, across, hidden, out_ref, cot_ref, rows_ref, cot_sem, row_sem):
+    tokens = own.shape[0]
+    core = order_ref[GROUP]
+
+    def fetch(k, source):
+        spot = pl.ds(k * tokens, tokens)
+        return pltpu.make_async_copy(source, cot_ref.at[spot], cot_sem.at[k])
+
+    def fetch_rows(k):
+        spot = pl.ds(k * tokens, tokens)
+        return pltpu.make_async_copy(hidden.at[order_ref[k]], rows_ref.at[spot], row_sem.at[k])
+
+    blocks = [fetch(0, own), fetch(1, side), fetch(2, across.at[0])]
+    for k, copy in enumerate(blocks):
+        copy.start()
+        fetch_rows(k).start()
+
+    @pl.when(core == 0)
     def _():
-        part = lax.dot_general(
-            across_ref[0], hidden_ref[0], (((0,), (0,)), ((), ())), preferred_element_type=F32
+        fetch(3, far).start()
+
+    @pl.when(core != 0)
+    def _():
+        fetch(3, across.at[1]).start()
+
+    fetch_rows(3).start()
+    total = None
+    for part in range(2):
+        for k in (2 * part, 2 * part + 1):
+            fetch(k, own).wait()
+            fetch_rows(k).wait()
+        span = slice(2 * part * tokens, 2 * (part + 1) * tokens)
+        value = lax.dot_general(
+            cot_ref[span], rows_ref[span], (((0,), (0,)), ((), ())), preferred_element_type=F32
         )
-        total_ref[...] += part
-
-    @pl.when(step == pl.num_programs(0) - 1)
-    def _():
-        out_ref[...] = total_ref[...].astype(BF16).reshape(out_ref.shape)
+        total = value if total is None else total + value
+    out_ref[...] = total.astype(BF16).reshape(out_ref.shape)
 
 
 def grad_of(order, own, side, far, across, hidden, n_rep):
     tokens, depth = own.shape
     block = hidden.shape[2]
-    shape = (n_rep, depth // n_rep, block)
-    same = pl.BlockSpec((tokens, depth), lambda i, order: (0, 0))
     return call(
         grad_body,
-        jax.ShapeDtypeStruct(shape, BF16),
+        jax.ShapeDtypeStruct((n_rep, depth // n_rep, block), BF16),
         flops=2 * GROUP * tokens * depth * block,
         limit=60,
-        grid_spec=pltpu.PrefetchScalarGridSpec(
-            num_scalar_prefetch=1,
-            grid=(GROUP + 1,),
-            in_specs=[same] * 3
-            + [
-                pl.BlockSpec(
-                    (1, tokens, depth), lambda i, order: (jnp.maximum(i - 3, 0), 0, 0)
-                ),
-                pl.BlockSpec((1, tokens, block), lambda i, order: (order[i], 0, 0)),
-            ],
-            out_specs=pl.BlockSpec(shape, lambda i, order: (0, 0, 0)),
-            scratch_shapes=[pltpu.VMEM((depth, block), F32)],
-        ),
+        in_specs=[pl.BlockSpec(memory_space=pltpu.SMEM)] + [pl.BlockSpec(memory_space=pl.ANY)] * 5,
+        out_specs=pl.BlockSpec(memory_space=pltpu.VMEM),
+        scratch_shapes=[
+            pltpu.VMEM((GROUP * tokens, depth), BF16),
+            pltpu.VMEM((GROUP * tokens, block), BF16),
+            pltpu.SemaphoreType.DMA((GROUP,)),
+            pltpu.SemaphoreType.DMA((GROUP,)),
+        ],
     )(order, own, side, far, across, hidden)
 
 
 def share_body(scale, parts_ref, taps_ref, grad_ref, small_ref):
     block = parts_ref.shape[2]
-    copies, rows, width = small_ref.shape
+    rows, width = taps_ref.shape
+    copies = small_ref.shape[0] // GROUP
     for zl in range(2):
         for yl in range(2):
             total = None
@@ -177,8 +187,13 @@
     norm = jnp.sum(value * value, axis=0, keepdims=True)
     row = lax.broadcasted_iota(jnp.int32, (rows, width), 0)
     small = jnp.where(row == rows - 1, norm, taps_ref[...]).astype(BF16)
-    for k in range(copies):
-        small_ref[k] = small
+    for member in range(GROUP):
+        start = member * block
+        size = min(block, width - start)
+        for k in range(member * copies, (member + 1) * copies):
+            small_ref[k, :, :size] = small[:, start : start + size]
+            if size < block:
+                small_ref[k, :, size:] = jnp.zeros((rows, block - size), BF16)
 
 
 def chain_body(rows, *refs):
@@ -253,16 +268,20 @@
 
 
 def middle_body(seen_ref, small_ref):
-    total = total_of(seen_ref).astype(BF16)
+    total = total_of(seen_ref).astype(small_ref.dtype)
     for k in range(small_ref.shape[0]):
         small_ref[k] = total
 
 
 def last_body(scale, seen_ref, gate_ref, up_ref, norm_ref):
-    total = total_of(seen_ref)
-    gate_ref[...] = total[:3] * scale
-    up_ref[...] = total[3:6] * scale
-    norm_ref[...] = total[7:] / D
+    block = seen_ref.shape[2]
+    for member in range(GROUP):
+        start = member * block
+        size = min(block, gate_ref.shape[1] - start)
+        lanes = slice(start, start + size)
+        gate_ref[:, lanes] = seen_ref[member, :3, :size] * scale
+        up_ref[:, lanes] = seen_ref[member, 3:6, :size] * scale
+        norm_ref[:, lanes] = seen_ref[member, 7:, :size] / D
 
 
 def local(gate_pre, up_pre, gate_taps, up_taps, down_weight, cotangent):
@@ -290,7 +309,7 @@
     tp = lax.axis_index("tp")
     member = lax.axis_index("zl") * 2 + lax.axis_index("yl")
     order = jnp.stack(
-        [member, member ^ (2 - tp), member ^ 3, member ^ (1 + tp), member ^ 3]
+        [member, member ^ (2 - tp), member ^ (1 + tp), member ^ 3, tp]
     )
 
     hidden = hidden_of(gate_pre, up_pre, before, gate_taps, up_taps, block, n_fs)
@@ -314,17 +333,17 @@
         terms, gate_pre, up_pre, before, after, gate_taps, up_taps, block
     )
 
-    wide = jax.ShapeDtypeStruct((8, width), F32)
-    sent = functools.partial(jax.ShapeDtypeStruct, dtype=BF16)
+    sent = jax.ShapeDtypeStruct((n_near, 8, block), BF16)
     grad_share, small = call(
-        functools.partial(share_body, grad_scale), (wide, sent((n_near, 8, width)))
+        functools.partial(share_body, grad_scale), (jax.ShapeDtypeStruct((8, width), F32), sent)
     )(parts, taps)
-    small = call(middle_body, sent((n_far, 8, width)))(swap(small, NEAR))
+    small = call(middle_body, jax.ShapeDtypeStruct((n_far, 8, block), BF16))(swap(small, NEAR))
+    small = call(middle_body, jax.ShapeDtypeStruct((GROUP, 8, block), F32))(swap(small, FAR))
     three = jax.ShapeDtypeStruct((3, width), F32)
     gate_out, up_out, norms = call(
         functools.partial(last_body, grad_scale),
         (three, three, jax.ShapeDtypeStruct((1, width), F32)),
-    )(swap(small, FAR))
+    )(swap(small, ("zl", "yl")))
     return grad_gate, grad_up, gate_out, up_out, grad_share[None], norms[0]
 
 

time: 166 us -> 167 us (level)
  the two profiles are of different devices: /device:TPU:16 before, /device:TPU:8 now
where the time goes in v1:
time: 167 us; the launch traced here: 166 us
  waiting for transfers between devices  51.4 us (31%)
  starting transfers between devices  46.1 us (28%)
  blocking collectives  41.4 us (25%)
  Pallas kernels  18.6 us (11%)
  local copies, waits for them, and re-layouts  6.12 us (4%)
  other arithmetic  2.04 us (1%)
    all_to_all x3, blocking collectives, swap(): return lax.all_to_all(array, axes, 0, 0, tiled=True)  41.4 us
    ppermute x1, waiting for transfers between devices, local(): side = lax.ppermute(cotangent, axes, first)  31.2 us
    all_to_all x2, starting transfers between devices, swap(): return lax.all_to_all(array, axes, 0, 0, tiled=True)  23.4 us
    ppermute x2, waiting for transfers between devices, passed_along(): return lax.ppermute(array, axis, pairs)  17.4 us
    ppermute x3, starting transfers between devices, local(): terms[k] = lax.ppermute(terms[k], 'fs', pairs)  10.7 us
    pallas_call x1, Pallas kernels, grad_of(): call(grad_body, jax.ShapeDtypeStruct((n_rep, depth // n_rep, block), BF16...  5.42 us
    pallas_call x1, Pallas kernels, chain_of(): call(functools.partial(chain_body, rows), (grad, grad, jax.ShapeDtypeStru...  5.13 us
    unnamed x26, local copies, waits for them, and re-layouts  4.72 us
  transfers between devices with their start and end apart: 10, of which 4 were waited for; matrix products, arithmetic and copies ran while one was open for 1% of the time, Pallas kernels for 5%

profile of v1, /device:TPU:8, one launch (start us, length us, event | category | flops | bytes accessed | tf_op | source)
XLA Modules:
  0.0 166.5 jit_solution(15901688334604783766)
XLA Ops:
  0.6 0.8 slice_bitcast_fusion
  1.5 3.4 %collective-permute-start = (bf16[2,2,1408]{2,1,0:T(2,128)(2,1)S(1)}, bf16[2,2,1408]{2,1,0:T(2,128)(2,1)S(1)}, u32[]{:S(2)}, u32[]{:S(2)}) collective-permute-start(bf16[2,2,1408]{2,1,0:T(2,128)(2,1)S(1)} %pad_maximum_fusion.1), channel_id=1, source_target_pairs={{0,2},{2,4},{4,6},{1,3},{3,5},{5,7},{8,10},{10,12},{12,14},{9,11},... | collective-permute-start | bytes 33800 | tf_op jit(solution)/shard_map/ppermute | solution.py:28
  4.9 1.4 collective-permute-done.before_ref.refs_6_
  6.3 0.6 copy-done.11
  6.9 4.2 %shard_map.109 = bf16[4,4,160,384]{3,2,1,0:T(8,128)(2,1)} custom-call(bf16[160,1408]{1,0:T(8,128)(2,1)} %refs_4_.1, bf16[160,1408]{1,0:T(8,128)(2,1)} %refs_5_.1, bf16[2,2,1408]{2,1,0:T(2,128)(2,1)} %copy-done.11, bf16[3,1408]{1,0:T(4,128)(2,1)} %refs_8_.1, bf16[3,1408]{1,0:T(4,128)(2,1)} %refs_9_.1), custom_call_target="tpu_custom_call" | custom-call | flops 9011200 | bytes 1048576 | tf_op jit(solution)/shard_map/pallas_call | solution.py:71
  11.1 8.5 %all-to-all-start = ((bf16[16,160,384]{2,1,0:T(8,128)(2,1)}), bf16[16,160,384]{2,1,0:T(8,128)(2,1)S(1)}, u32[]{:S(2)}, u32[]{:S(2)}) async-start(bf16[16,160,384]{2,1,0:T(8,128)(2,1)} %bitcast.23), calls=%async_computation | async-start | bytes 3932160 | tf_op jit(solution)/shard_map/all_to_all | solution.py:32
  19.6 3.4 %collective-permute-start.5 = (bf16[640,512]{1,0:T(8,128)(2,1)S(1)}, bf16[640,512]{1,0:T(8,128)(2,1)S(1)}, u32[]{:S(2)}, u32[]{:S(2)}) collective-permute-start(bf16[640,512]{1,0:T(8,128)(2,1)S(1)} %copy-done), channel_id=1, source_target_pairs={{0,64},{1,9},{8,72},{9,1},{64,0},{65,73},{72,8},{73,65},{2,66},{3,... | collective-permute-start | bytes 1966088 | tf_op jit(solution)/shard_map/ppermute | solution.py:306
  23.0 2.0 %collective-permute-start.6 = (bf16[640,512]{1,0:T(8,128)(2,1)S(1)}, bf16[640,512]{1,0:T(8,128)(2,1)S(1)}, u32[]{:S(2)}, u32[]{:S(2)}) collective-permute-start(bf16[640,512]{1,0:T(8,128)(2,1)S(1)} %copy-done), channel_id=1, source_target_pairs={{0,72},{8,64},{64,8},{72,0},{2,74},{10,66},{66,10},{74,2},{4,76},{... | collective-permute-start | bytes 1966088 | tf_op jit(solution)/shard_map/ppermute | solution.py:307
  25.0 31.2 %collective-permute-done.5.side = bf16[640,512]{1,0:T(8,128)(2,1)S(1)} collective-permute-done((bf16[640,512]{1,0:T(8,128)(2,1)S(1)}, bf16[640,512]{1,0:T(8,128)(2,1)S(1)}, u32[]{:S(2)}, u32[]{:S(2)}) %collective-permute-start.5) | collective-permute-done | bytes 655392 | tf_op jit(solution)/shard_map/ppermute | solution.py:306
  56.3 1.3 pad_maximum_fusion
  57.7 1.9 %collective-permute-start.7 = (bf16[2,640,512]{2,1,0:T(8,128)(2,1)}, bf16[2,640,512]{2,1,0:T(8,128)(2,1)}, u32[]{:S(2)}, u32[]{:S(2)}) collective-permute-start(bf16[2,640,512]{2,1,0:T(8,128)(2,1)} %pad_maximum_fusion), channel_id=1, source_target_pairs={{0,1},{1,0},{2,3},{3,2},{4,5},{5,4},{6,7},{7,6},{8,9},{9,8},{10,11... | collective-permute-start | bytes 3932168 | tf_op jit(solution)/shard_map/ppermute | solution.py:308
  59.6 0.6 stack.76.order_ref
  60.2 2.7 %collective-permute-done.7.across = bf16[2,640,512]{2,1,0:T(8,128)(2,1)} collective-permute-done((bf16[2,640,512]{2,1,0:T(8,128)(2,1)}, bf16[2,640,512]{2,1,0:T(8,128)(2,1)}, u32[]{:S(2)}, u32[]{:S(2)}) %collective-permute-start.7) | collective-permute-done | bytes 1310752 | tf_op jit(solution)/shard_map/ppermute | solution.py:308
  63.0 1.3 copy-done.5
  64.3 5.4 %shard_map.112 = bf16[64,8,384]{2,1,0:T(8,128)(2,1)} custom-call(s32[5]{0:T(128)} %stack.76.order_ref, bf16[640,512]{1,0:T(8,128)(2,1)} %own.1, bf16[640,512]{1,0:T(8,128)(2,1)} %copy-done.6, bf16[640,512]{1,0:T(8,128)(2,1)} %copy-done.7, bf16[2,640,512]{2,1,0:T(8,128)(2,1)} %collective-permute-done.7.across, bf16[4,640,384]{2,1,0:T(8,128)(2,1)} %bitcast.22), custom_call_target="tpu_custom_call" | custom-call | flops 1006632960 | bytes 1048576 | tf_op jit(solution)/shard_map/pallas_call | solution.py:156
  69.7 14.9 %all-to-all-start.1 = ((bf16[64,8,384]{2,1,0:T(8,128)(2,1)}), bf16[64,8,384]{2,1,0:T(8,128)(2,1)S(1)}, u32[]{:S(2)}, u32[]{:S(2)}) async-start(bf16[64,8,384]{2,1,0:T(8,128)(2,1)} %shard_map.112), calls=%async_computation.1 | async-start | bytes 786432 | tf_op jit(solution)/shard_map/all_to_all | solution.py:32
  84.7 2.4 %shard_map.110 = (bf16[168,1408]{1,0:T(8,128)(2,1)S(1)}, bf16[168,1408]{1,0:T(8,128)(2,1)S(1)}, bf16[168,1408]{1,0:T(8,128)(2,1)S(1)}, bf16[168,1408]{1,0:T(8,128)(2,1)S(1)}) custom-call(s32[4]{0:T(128)S(1)} %pad_add_fusion.at_ref, bf16[640,512]{1,0:T(8,128)(2,1)S(1)} %copy-done.1, bf16[1408,512]{1,0:T(8,128)(2,1)S(1)} %copy-done.4), custom_call_target="tpu_custom_call" | custom-call | flops 922746880 | bytes 1048576 | tf_op jit(solution)/shard_map/pallas_call | solution.py:103
  87.2 0.8 copy-done.2
  88.0 3.7 %collective-permute-start.1 = (bf16[168,1408]{1,0:T(8,128)(2,1)S(1)}, bf16[168,1408]{1,0:T(8,128)(2,1)S(1)}, u32[]{:S(2)}, u32[]{:S(2)}) collective-permute-start(bf16[168,1408]{1,0:T(8,128)(2,1)S(1)} %get-tuple-element.20), channel_id=1, source_target_pairs={{0,2},{2,4},{4,6},{6,0},{1,3},{3,5},{5,7},{7,1},{8,10},{10,12},{12... | collective-permute-start | bytes 1419272 | tf_op jit(solution)/shard_map/ppermute | solution.py:325
  91.7 3.3 %collective-permute-start.2 = (bf16[168,1408]{1,0:T(8,128)(2,1)S(1)}, bf16[168,1408]{1,0:T(8,128)(2,1)S(1)}, u32[]{:S(2)}, u32[]{:S(2)}) collective-permute-start(bf16[168,1408]{1,0:T(8,128)(2,1)S(1)} %get-tuple-element.21), channel_id=1, source_target_pairs={{0,6},{2,0},{4,2},{6,4},{1,7},{3,1},{5,3},{7,5},{8,14},{10,8},{12,... | collective-permute-start | bytes 1419272 | tf_op jit(solution)/shard_map/ppermute | solution.py:325
  95.0 3.7 %collective-permute-start.3 = (bf16[168,1408]{1,0:T(8,128)(2,1)S(1)}, bf16[168,1408]{1,0:T(8,128)(2,1)S(1)}, u32[]{:S(2)}, u32[]{:S(2)}) collective-permute-start(bf16[168,1408]{1,0:T(8,128)(2,1)S(1)} %get-tuple-element.22), channel_id=1, source_target_pairs={{0,4},{2,6},{4,0},{6,2},{1,5},{3,7},{5,1},{7,3},{8,12},{10,14},{12... | collective-permute-start | bytes 1419272 | tf_op jit(solution)/shard_map/ppermute | solution.py:325
  98.7 1.3 collective-permute-start.4
  100.0 16.0 %collective-permute-done.4.refs_7_ = bf16[2,2,1408]{2,1,0:T(2,128)(2,1)S(1)} collective-permute-done((bf16[2,2,1408]{2,1,0:T(2,128)(2,1)S(1)}, bf16[2,2,1408]{2,1,0:T(2,128)(2,1)S(1)}, u32[]{:S(2)}, u32[]{:S(2)}) %collective-permute-start.4) | collective-permute-done | bytes 11296 | tf_op jit(solution)/shard_map/ppermute | solution.py:28
  116.1 0.6 copy-done.12
  117.1 5.1 %shard_map.111 = (bf16[160,1408]{1,0:T(8,128)(2,1)}, bf16[160,1408]{1,0:T(8,128)(2,1)}, f32[8,1408]{1,0:T(8,128)}) custom-call(bf16[168,1408]{1,0:T(8,128)(2,1)} %copy-done.8, bf16[168,1408]{1,0:T(8,128)(2,1)} %copy-done.9, bf16[168,1408]{1,0:T(8,128)(2,1)} %copy-done.10, bf16[168,1408]{1,0:T(8,128)(2,1)} %copy-done.2, bf16[160,1408]{1,0:T(8,128)(2,1)} %refs_4_.1, ...), custom_call_target="tpu_custom_call" | custom-call | flops 22528000 | bytes 1048576 | tf_op jit(solution)/shard_map/pallas_call | solution.py:249
  122.3 0.8 copy-done.3
  123.1 0.7 shard_map.113
  123.7 11.6 %all_to_all.25.seen_ref = bf16[16,8,384]{2,1,0:T(8,128)(2,1)S(1)} all-to-all(bf16[16,8,384]{2,1,0:T(8,128)(2,1)S(1)} %get-tuple-element.27), channel_id=1, replica_groups=mesh['zh'=4,'zl'=2,'yh'=4,'yl'=2,'fs'=4,'tp'=2] {'zl','yl','fs'}, dimensions={0} | all-to-all | bytes 196608 | tf_op jit(solution)/shard_map/all_to_all | solution.py:32
  135.3 22.2 %all_to_all.26.seen_ref = bf16[16,8,384]{2,1,0:T(8,128)(2,1)S(1)} all-to-all(bf16[16,8,384]{2,1,0:T(8,128)(2,1)S(1)} %shard_map.114), channel_id=1, replica_groups=mesh['zh'=4,'zl'=2,'yh'=4,'yl'=2,'fs'=4,'tp'=2] {'zh','yh'}, dimensions={0} | all-to-all | bytes 196608 | tf_op jit(solution)/shard_map/all_to_all | solution.py:32
  157.6 7.6 %all_to_all.27.seen_ref = f32[4,8,384]{2,1,0:T(8,128)S(1)} all-to-all(f32[4,8,384]{2,1,0:T(8,128)S(1)} %shard_map.115), channel_id=1, replica_groups=mesh['zh'=4,'zl'=2,'yh'=4,'yl'=2,'fs'=4,'tp'=2] {'zl','yl'}, dimensions={0} | all-to-all | bytes 98304 | tf_op jit(solution)/shard_map/all_to_all | solution.py:32
  165.2 0.6 shard_map.116
  165.8 0.6 reduce
  (32 shorter events, 0.9 us)
Async XLA Ops:
  1.5 4.8 %collective-permute-start = (bf16[2,2,1408]{2,1,0:T(2,128)(2,1)S(1)}, bf16[2,2,1408]{2,1,0:T(2,128)(2,1)S(1)}, u32[]{:S(2)}, u32[]{:S(2)}) collective-permute-start(bf16[2,2,1408]{2,1,0:T(2,128)(2,1)S(1)} %pad_maximum_fusion.1), channel_id=1, source_target_pairs={{0,2},{2,4},{4,6},{1,3},{3,5},{5,7},{8,10},{10,12},{12,14},{9,11},... | collective-permute-start | bytes 33800 | tf_op jit(solution)/shard_map/ppermute | solution.py:28
  6.3 0.6 copy-start.11
  11.1 8.5 %copy-start = (bf16[640,512]{1,0:T(8,128)(2,1)S(1)}, bf16[640,512]{1,0:T(8,128)(2,1)}, u32[]{:S(2)}) copy-start(bf16[640,512]{1,0:T(8,128)(2,1)} %own.1) | copy-start | bytes 1966084
  11.1 51.9 %all-to-all-start = ((bf16[16,160,384]{2,1,0:T(8,128)(2,1)}), bf16[16,160,384]{2,1,0:T(8,128)(2,1)S(1)}, u32[]{:S(2)}, u32[]{:S(2)}) async-start(bf16[16,160,384]{2,1,0:T(8,128)(2,1)} %bitcast.23), calls=%async_computation | async-start | bytes 3932160 | tf_op jit(solution)/shard_map/all_to_all | solution.py:32
  19.6 36.6 %collective-permute-start.5 = (bf16[640,512]{1,0:T(8,128)(2,1)S(1)}, bf16[640,512]{1,0:T(8,128)(2,1)S(1)}, u32[]{:S(2)}, u32[]{:S(2)}) collective-permute-start(bf16[640,512]{1,0:T(8,128)(2,1)S(1)} %copy-done), channel_id=1, source_target_pairs={{0,64},{1,9},{8,72},{9,1},{64,0},{65,73},{72,8},{73,65},{2,66},{3,... | collective-permute-start | bytes 1966088 | tf_op jit(solution)/shard_map/ppermute | solution.py:306
  23.0 33.3 %collective-permute-start.6 = (bf16[640,512]{1,0:T(8,128)(2,1)S(1)}, bf16[640,512]{1,0:T(8,128)(2,1)S(1)}, u32[]{:S(2)}, u32[]{:S(2)}) collective-permute-start(bf16[640,512]{1,0:T(8,128)(2,1)S(1)} %copy-done), channel_id=1, source_target_pairs={{0,72},{8,64},{64,8},{72,0},{2,74},{10,66},{66,10},{74,2},{4,76},{... | collective-permute-start | bytes 1966088 | tf_op jit(solution)/shard_map/ppermute | solution.py:307
  56.3 1.3 copy-start.6
  56.3 1.5 copy-start.7
  57.7 5.3 %collective-permute-start.7 = (bf16[2,640,512]{2,1,0:T(8,128)(2,1)}, bf16[2,640,512]{2,1,0:T(8,128)(2,1)}, u32[]{:S(2)}, u32[]{:S(2)}) collective-permute-start(bf16[2,640,512]{2,1,0:T(8,128)(2,1)} %pad_maximum_fusion), channel_id=1, source_target_pairs={{0,1},{1,0},{2,3},{3,2},{4,5},{5,4},{6,7},{7,6},{8,9},{9,8},{10,11... | collective-permute-start | bytes 3932168 | tf_op jit(solution)/shard_map/ppermute | solution.py:308
  63.0 1.3 copy-start.5
  64.3 20.5 %copy-start.1 = (bf16[640,512]{1,0:T(8,128)(2,1)S(1)}, bf16[640,512]{1,0:T(8,128)(2,1)}, u32[]{:S(2)}) copy-start(bf16[640,512]{1,0:T(8,128)(2,1)} %own.1) | copy-start | bytes 1966084
  64.3 20.5 %copy-start.4 = (bf16[1408,512]{1,0:T(8,128)(2,1)S(1)}, bf16[1408,512]{1,0:T(8,128)(2,1)}, u32[]{:S(2)}) copy-start(bf16[1408,512]{1,0:T(8,128)(2,1)} %weight_ref.1) | copy-start | bytes 4325380
  69.7 52.5 %all-to-all-start.1 = ((bf16[64,8,384]{2,1,0:T(8,128)(2,1)}), bf16[64,8,384]{2,1,0:T(8,128)(2,1)S(1)}, u32[]{:S(2)}, u32[]{:S(2)}) async-start(bf16[64,8,384]{2,1,0:T(8,128)(2,1)} %shard_map.112), calls=%async_computation.1 | async-start | bytes 786432 | tf_op jit(solution)/shard_map/all_to_all | solution.py:32
  87.2 0.8 copy-start.2
  88.0 28.1 %collective-permute-start.1 = (bf16[168,1408]{1,0:T(8,128)(2,1)S(1)}, bf16[168,1408]{1,0:T(8,128)(2,1)S(1)}, u32[]{:S(2)}, u32[]{:S(2)}) collective-permute-start(bf16[168,1408]{1,0:T(8,128)(2,1)S(1)} %get-tuple-element.20), channel_id=1, source_target_pairs={{0,2},{2,4},{4,6},{6,0},{1,3},{3,5},{5,7},{7,1},{8,10},{10,12},{12... | collective-permute-start | bytes 1419272 | tf_op jit(solution)/shard_map/ppermute | solution.py:325
  91.7 24.3 %collective-permute-start.2 = (bf16[168,1408]{1,0:T(8,128)(2,1)S(1)}, bf16[168,1408]{1,0:T(8,128)(2,1)S(1)}, u32[]{:S(2)}, u32[]{:S(2)}) collective-permute-start(bf16[168,1408]{1,0:T(8,128)(2,1)S(1)} %get-tuple-element.21), channel_id=1, source_target_pairs={{0,6},{2,0},{4,2},{6,4},{1,7},{3,1},{5,3},{7,5},{8,14},{10,8},{12,... | collective-permute-start | bytes 1419272 | tf_op jit(solution)/shard_map/ppermute | solution.py:325
  95.0 21.0 %collective-permute-start.3 = (bf16[168,1408]{1,0:T(8,128)(2,1)S(1)}, bf16[168,1408]{1,0:T(8,128)(2,1)S(1)}, u32[]{:S(2)}, u32[]{:S(2)}) collective-permute-start(bf16[168,1408]{1,0:T(8,128)(2,1)S(1)} %get-tuple-element.22), channel_id=1, source_target_pairs={{0,4},{2,6},{4,0},{6,2},{1,5},{3,7},{5,1},{7,3},{8,12},{10,14},{12... | collective-permute-start | bytes 1419272 | tf_op jit(solution)/shard_map/ppermute | solution.py:325
  98.7 17.3 %collective-permute-start.4 = (bf16[2,2,1408]{2,1,0:T(2,128)(2,1)S(1)}, bf16[2,2,1408]{2,1,0:T(2,128)(2,1)S(1)}, u32[]{:S(2)}, u32[]{:S(2)}) collective-permute-start(bf16[2,2,1408]{2,1,0:T(2,128)(2,1)S(1)} %pad_maximum_fusion.2), channel_id=1, source_target_pairs={{2,0},{4,2},{6,4},{3,1},{5,3},{7,5},{10,8},{12,10},{14,12},{11,9},... | collective-permute-start | bytes 33800 | tf_op jit(solution)/shard_map/ppermute | solution.py:28
  116.0 0.6 copy-start.12
  116.0 0.8 copy-start.8
  116.0 0.9 copy-start.9
  116.1 1.1 copy-start.10
  122.3 0.8 copy-start.3

commit v2 on v1

--- a/solution.py
+++ b/solution.py
@@ -111,62 +111,82 @@
     )(at, cotangent, weight)
 
 
-def grad_body(order_ref, own, side, far, across, hidden, out_ref, cot_ref, rows_ref, cot_sem, row_sem):
-    tokens = own.shape[0]
-    core = order_ref[GROUP]
-
-    def fetch(k, source):
-        spot = pl.ds(k * tokens, tokens)
-        return pltpu.make_async_copy(source, cot_ref.at[spot], cot_sem.at[k])
+def turn_body(core_ref, own_ref, side_ref, far_ref, across_ref, out_ref):
+    step = pl.program_id(0)
+    core = core_ref[0]
+    cases = (
+        (step == 0, lambda: own_ref[...]),
+        (step == 1, lambda: side_ref[...]),
+        (step == 2, lambda: across_ref[0]),
+        ((step == 3) & (core == 0), lambda: far_ref[...]),
+        ((step == 3) & (core != 0), lambda: across_ref[1]),
+    )
+    for case, block in cases:
+
+        @pl.when(case)
+        def _(block=block):
+            out_ref[...] = block().T
+
+
+def turn_of(core, own, side, far, across):
+    tokens, depth = own.shape
+    same = pl.BlockSpec((tokens, depth), lambda i: (0, 0))
+    return call(
+        turn_body,
+        jax.ShapeDtypeStruct((depth, GROUP * tokens), BF16),
+        flops=tokens * depth,
+        limit=60,
+        grid=(GROUP,),
+        in_specs=[pl.BlockSpec(memory_space=pltpu.SMEM)]
+        + [same] * 3
+        + [pl.BlockSpec((2, tokens, depth), lambda i: (0, 0, 0))],
+        out_specs=pl.BlockSpec((depth, tokens), lambda i: (0, i)),
+    )(core, own, side, far, across)
+
+
+def grad_body(order_ref, turned, hidden, out_ref, cot_ref, rows_ref, cot_sem, row_sem):
+    tokens = hidden.shape[1]
+
+    def fetch(part):
+        spot = pl.ds(2 * part * tokens, 2 * tokens)
+        return pltpu.make_async_copy(turned.at[:, spot], cot_ref.at[:, spot], cot_sem.at[part])
 
     def fetch_rows(k):
         spot = pl.ds(k * tokens, tokens)
         return pltpu.make_async_copy(hidden.at[order_ref[k]], rows_ref.at[spot], row_sem.at[k])
 
-    blocks = [fetch(0, own), fetch(1, side), fetch(2, across.at[0])]
-    for k, copy in enumerate(blocks):
-        copy.start()
-        fetch_rows(k).start()
-
-    @pl.when(core == 0)
-    def _():
-        fetch(3, far).start()
-
-    @pl.when(core != 0)
-    def _():
-        fetch(3, across.at[1]).start()
-
-    fetch_rows(3).start()
+    for part in range(2):
+        fetch(part).start()
+        fetch_rows(2 * part).start()
+        fetch_rows(2 * part + 1).start()
     total = None
     for part in range(2):
-        for k in (2 * part, 2 * part + 1):
-            fetch(k, own).wait()
-            fetch_rows(k).wait()
+        fetch(part).wait()
+        fetch_rows(2 * part).wait()
+        fetch_rows(2 * part + 1).wait()
         span = slice(2 * part * tokens, 2 * (part + 1) * tokens)
-        value = lax.dot_general(
-            cot_ref[span], rows_ref[span], (((0,), (0,)), ((), ())), preferred_element_type=F32
-        )
+        value = jnp.dot(cot_ref[:, span], rows_ref[span], preferred_element_type=F32)
         total = value if total is None else total + value
     out_ref[...] = total.astype(BF16).reshape(out_ref.shape)
 
 
-def grad_of(order, own, side, far, across, hidden, n_rep):
-    tokens, depth = own.shape
+def grad_of(order, turned, hidden, n_rep):
+    depth, tokens = turned.shape
     block = hidden.shape[2]
     return call(
         grad_body,
         jax.ShapeDtypeStruct((n_rep, depth // n_rep, block), BF16),
-        flops=2 * GROUP * tokens * depth * block,
+        flops=2 * tokens * depth * block,
         limit=60,
-        in_specs=[pl.BlockSpec(memory_space=pltpu.SMEM)] + [pl.BlockSpec(memory_space=pl.ANY)] * 5,
+        in_specs=[pl.BlockSpec(memory_space=pltpu.SMEM)] + [pl.BlockSpec(memory_space=pl.ANY)] * 2,
         out_specs=pl.BlockSpec(memory_space=pltpu.VMEM),
         scratch_shapes=[
-            pltpu.VMEM((GROUP * tokens, depth), BF16),
-            pltpu.VMEM((GROUP * tokens, block), BF16),
-            pltpu.SemaphoreType.DMA((GROUP,)),
+            pltpu.VMEM((depth, tokens), BF16),
+            pltpu.VMEM((tokens, block), BF16),
+            pltpu.SemaphoreType.DMA((2,)),
             pltpu.SemaphoreType.DMA((GROUP,)),
         ],
-    )(order, own, side, far, across, hidden)
+    )(order, turned, hidden)
 
 
 def share_body(scale, parts_ref, taps_ref, grad_ref, small_ref):
@@ -309,8 +329,10 @@
     tp = lax.axis_index("tp")
     member = lax.axis_index("zl") * 2 + lax.axis_index("yl")
     order = jnp.stack(
-        [member, member ^ (2 - tp), member ^ (1 + tp), member ^ 3, tp]
-    )
+        [member, member ^ (2 - tp), member ^ (1 + tp), member ^ 3]
+    )
+
+    turned = turn_of(tp[None], cotangent, side, far, across)
 
     hidden = hidden_of(gate_pre, up_pre, before, gate_taps, up_taps, block, n_fs)
     everyone = swap(hidden.reshape(n_near, rows, block), NEAR)
@@ -324,9 +346,7 @@
         pairs = [(i, (i + step) % n_fs) for i in range(n_fs)]
         terms[k] = lax.ppermute(terms[k], "fs", pairs)
 
-    partial = grad_of(
-        order, cotangent, side, far, across, everyone.reshape(GROUP, -1, block), n_rep
-    )
+    partial = grad_of(order, turned, everyone.reshape(GROUP, -1, block), n_rep)
     parts = swap(partial, ZY)
 
     grad_gate, grad_up, taps = chain_of(
@@ -335,7 +355,8 @@
 
     sent = jax.ShapeDtypeStruct((n_near, 8, block), BF16)
     grad_share, small = call(
-        functools.partial(share_body, grad_scale), (jax.ShapeDtypeStruct((8, width), F32), sent)
+        functools.partial(share_body, grad_scale),
+        (jax.ShapeDtypeStruct((8, width), F32), sent),
     )(parts, taps)
     small = call(middle_body, jax.ShapeDtypeStruct((n_far, 8, block), BF16))(swap(small, NEAR))
     small = call(middle_body, jax.ShapeDtypeStruct((GROUP, 8, block), F32))(swap(small, FAR))

time: 167 us -> 172 us (1.030)
  Pallas kernels: 18.6 us -> 22.9 us
    pallas_call x0 -> x1, Pallas kernels: none -> 4.42 us  [turn_of(): call(turn_body, jax.ShapeDtypeStruct((depth, GROUP * tokens), BF16), flop...]
  transfers between devices with their start and end apart: 10 -> 10, of which waited for: 4 -> 4; matrix products, arithmetic and copies ran while one was open for 1% -> 1% of each run, Pallas kernels for 5% -> 7%
where the time goes in v2:
time: 172 us; the launch traced here: 171 us
  waiting for transfers between devices  51.3 us (30%)
  starting transfers between devices  46.1 us (27%)
  blocking collectives  41.4 us (24%)
  Pallas kernels  22.9 us (13%)
  local copies, waits for them, and re-layouts  5.59 us (3%)
  other arithmetic  2.67 us (2%)
    all_to_all x3, blocking collectives, swap(): return lax.all_to_all(array, axes, 0, 0, tiled=True)  41.4 us
    ppermute x1, waiting for transfers between devices, local(): side = lax.ppermute(cotangent, axes, first)  31.2 us
    all_to_all x2, starting transfers between devices, swap(): return lax.all_to_all(array, axes, 0, 0, tiled=True)  23.4 us
    ppermute x2, waiting for transfers between devices, passed_along(): return lax.ppermute(array, axis, pairs)  17.4 us
    ppermute x3, starting transfers between devices, local(): terms[k] = lax.ppermute(terms[k], 'fs', pairs)  10.7 us
    pallas_call x1, Pallas kernels, grad_of(): call(grad_body, jax.ShapeDtypeStruct((n_rep, depth // n_rep, block), BF16...  5.37 us
    pallas_call x1, Pallas kernels, chain_of(): call(functools.partial(chain_body, rows), (grad, grad, jax.ShapeDtypeStru...  5.13 us
    unnamed x26, local copies, waits for them, and re-layouts  4.78 us
  transfers between devices with their start and end apart: 10, of which 4 were waited for; matrix products, arithmetic and copies ran while one was open for 1% of the time, Pallas kernels for 7%

profile of v2, /device:TPU:8, one launch (start us, length us, event | category | flops | bytes accessed | tf_op | source)
XLA Modules:
  0.0 170.8 jit_solution(13012218540128696935)
XLA Ops:
  0.6 0.8 slice_bitcast_fusion
  1.5 3.4 %collective-permute-start = (bf16[2,2,1408]{2,1,0:T(2,128)(2,1)S(1)}, bf16[2,2,1408]{2,1,0:T(2,128)(2,1)S(1)}, u32[]{:S(2)}, u32[]{:S(2)}) collective-permute-start(bf16[2,2,1408]{2,1,0:T(2,128)(2,1)S(1)} %pad_maximum_fusion.1), channel_id=1, source_target_pairs={{0,2},{2,4},{4,6},{1,3},{3,5},{5,7},{8,10},{10,12},{12,14},{9,11},... | collective-permute-start | bytes 33800 | tf_op jit(solution)/shard_map/ppermute | solution.py:28
  4.9 1.4 collective-permute-done.before_ref.refs_6_
  6.3 0.6 copy-done.11
  6.9 4.2 %shard_map.109 = bf16[4,4,160,384]{3,2,1,0:T(8,128)(2,1)} custom-call(bf16[160,1408]{1,0:T(8,128)(2,1)} %refs_4_.1, bf16[160,1408]{1,0:T(8,128)(2,1)} %refs_5_.1, bf16[2,2,1408]{2,1,0:T(2,128)(2,1)} %copy-done.11, bf16[3,1408]{1,0:T(4,128)(2,1)} %refs_8_.1, bf16[3,1408]{1,0:T(4,128)(2,1)} %refs_9_.1), custom_call_target="tpu_custom_call" | custom-call | flops 9011200 | bytes 1048576 | tf_op jit(solution)/shard_map/pallas_call | solution.py:71
  11.1 8.5 %all-to-all-start = ((bf16[16,160,384]{2,1,0:T(8,128)(2,1)}), bf16[16,160,384]{2,1,0:T(8,128)(2,1)S(1)}, u32[]{:S(2)}, u32[]{:S(2)}) async-start(bf16[16,160,384]{2,1,0:T(8,128)(2,1)} %bitcast.23), calls=%async_computation | async-start | bytes 3932160 | tf_op jit(solution)/shard_map/all_to_all | solution.py:32
  19.6 3.4 %collective-permute-start.5 = (bf16[640,512]{1,0:T(8,128)(2,1)S(1)}, bf16[640,512]{1,0:T(8,128)(2,1)S(1)}, u32[]{:S(2)}, u32[]{:S(2)}) collective-permute-start(bf16[640,512]{1,0:T(8,128)(2,1)S(1)} %copy-done), channel_id=1, source_target_pairs={{0,64},{1,9},{8,72},{9,1},{64,0},{65,73},{72,8},{73,65},{2,66},{3,... | collective-permute-start | bytes 1966088 | tf_op jit(solution)/shard_map/ppermute | solution.py:326
  23.0 2.0 %collective-permute-start.6 = (bf16[640,512]{1,0:T(8,128)(2,1)S(1)}, bf16[640,512]{1,0:T(8,128)(2,1)S(1)}, u32[]{:S(2)}, u32[]{:S(2)}) collective-permute-start(bf16[640,512]{1,0:T(8,128)(2,1)S(1)} %copy-done), channel_id=1, source_target_pairs={{0,72},{8,64},{64,8},{72,0},{2,74},{10,66},{66,10},{74,2},{4,76},{... | collective-permute-start | bytes 1966088 | tf_op jit(solution)/shard_map/ppermute | solution.py:327
  25.0 31.2 %collective-permute-done.5.side_ref = bf16[640,512]{1,0:T(8,128)(2,1)S(1)} collective-permute-done((bf16[640,512]{1,0:T(8,128)(2,1)S(1)}, bf16[640,512]{1,0:T(8,128)(2,1)S(1)}, u32[]{:S(2)}, u32[]{:S(2)}) %collective-permute-start.5) | collective-permute-done | bytes 655392 | tf_op jit(solution)/shard_map/ppermute | solution.py:326
  56.2 1.3 pad_maximum_fusion
  57.7 1.9 %collective-permute-start.7 = (bf16[2,640,512]{2,1,0:T(8,128)(2,1)}, bf16[2,640,512]{2,1,0:T(8,128)(2,1)}, u32[]{:S(2)}, u32[]{:S(2)}) collective-permute-start(bf16[2,640,512]{2,1,0:T(8,128)(2,1)} %pad_maximum_fusion), channel_id=1, source_target_pairs={{0,1},{1,0},{2,3},{3,2},{4,5},{5,4},{6,7},{7,6},{8,9},{9,8},{10,11... | collective-permute-start | bytes 3932168 | tf_op jit(solution)/shard_map/ppermute | solution.py:328
  59.6 0.6 pad_add_fusion.1.order_ref
  60.3 2.7 %collective-permute-done.7.across_ref = bf16[2,640,512]{2,1,0:T(8,128)(2,1)} collective-permute-done((bf16[2,640,512]{2,1,0:T(8,128)(2,1)}, bf16[2,640,512]{2,1,0:T(8,128)(2,1)}, u32[]{:S(2)}, u32[]{:S(2)}) %collective-permute-start.7) | collective-permute-done | bytes 1310752 | tf_op jit(solution)/shard_map/ppermute | solution.py:328
  63.0 4.4 %shard_map.112.turned = bf16[512,2560]{1,0:T(8,128)(2,1)} custom-call(s32[1]{0:T(128)} %bitcast.12.core_ref, bf16[640,512]{1,0:T(8,128)(2,1)} %own_ref.1, bf16[640,512]{1,0:T(8,128)(2,1)} %copy-done.6, bf16[640,512]{1,0:T(8,128)(2,1)} %copy-done.7, bf16[2,640,512]{2,1,0:T(8,128)(2,1)} %collective-permute-done.7.across_ref), custom_call_target="tpu_custom_call" | custom-call | flops 327680 | bytes 1048576 | tf_op jit(solution)/shard_map/pallas_call | solution.py:134
  67.4 1.3 copy-done.5
  68.7 5.4 %shard_map.113 = bf16[64,8,384]{2,1,0:T(8,128)(2,1)} custom-call(s32[4]{0:T(128)} %pad_add_fusion.1.order_ref, bf16[512,2560]{1,0:T(8,128)(2,1)} %shard_map.112.turned, bf16[4,640,384]{2,1,0:T(8,128)(2,1)} %bitcast.22), custom_call_target="tpu_custom_call" | custom-call | flops 1006632960 | bytes 1048576 | tf_op jit(solution)/shard_map/pallas_call | solution.py:176
  74.1 14.9 %all-to-all-start.1 = ((bf16[64,8,384]{2,1,0:T(8,128)(2,1)}), bf16[64,8,384]{2,1,0:T(8,128)(2,1)S(1)}, u32[]{:S(2)}, u32[]{:S(2)}) async-start(bf16[64,8,384]{2,1,0:T(8,128)(2,1)} %shard_map.113), calls=%async_computation.1 | async-start | bytes 786432 | tf_op jit(solution)/shard_map/all_to_all | solution.py:32
  89.1 2.4 %shard_map.110 = (bf16[168,1408]{1,0:T(8,128)(2,1)S(1)}, bf16[168,1408]{1,0:T(8,128)(2,1)S(1)}, bf16[168,1408]{1,0:T(8,128)(2,1)S(1)}, bf16[168,1408]{1,0:T(8,128)(2,1)S(1)}) custom-call(s32[4]{0:T(128)S(1)} %pad_add_fusion.at_ref, bf16[640,512]{1,0:T(8,128)(2,1)S(1)} %copy-done.1, bf16[1408,512]{1,0:T(8,128)(2,1)S(1)} %copy-done.4), custom_call_target="tpu_custom_call" | custom-call | flops 922746880 | bytes 1048576 | tf_op jit(solution)/shard_map/pallas_call | solution.py:103
  91.5 0.8 copy-done.2
  92.3 3.7 %collective-permute-start.1 = (bf16[168,1408]{1,0:T(8,128)(2,1)S(1)}, bf16[168,1408]{1,0:T(8,128)(2,1)S(1)}, u32[]{:S(2)}, u32[]{:S(2)}) collective-permute-start(bf16[168,1408]{1,0:T(8,128)(2,1)S(1)} %get-tuple-element.20), channel_id=1, source_target_pairs={{0,2},{2,4},{4,6},{6,0},{1,3},{3,5},{5,7},{7,1},{8,10},{10,12},{12... | collective-permute-start | bytes 1419272 | tf_op jit(solution)/shard_map/ppermute | solution.py:347
  96.1 3.3 %collective-permute-start.2 = (bf16[168,1408]{1,0:T(8,128)(2,1)S(1)}, bf16[168,1408]{1,0:T(8,128)(2,1)S(1)}, u32[]{:S(2)}, u32[]{:S(2)}) collective-permute-start(bf16[168,1408]{1,0:T(8,128)(2,1)S(1)} %get-tuple-element.21), channel_id=1, source_target_pairs={{0,6},{2,0},{4,2},{6,4},{1,7},{3,1},{5,3},{7,5},{8,14},{10,8},{12,... | collective-permute-start | bytes 1419272 | tf_op jit(solution)/shard_map/ppermute | solution.py:347
  99.4 3.6 %collective-permute-start.3 = (bf16[168,1408]{1,0:T(8,128)(2,1)S(1)}, bf16[168,1408]{1,0:T(8,128)(2,1)S(1)}, u32[]{:S(2)}, u32[]{:S(2)}) collective-permute-start(bf16[168,1408]{1,0:T(8,128)(2,1)S(1)} %get-tuple-element.22), channel_id=1, source_target_pairs={{0,4},{2,6},{4,0},{6,2},{1,5},{3,7},{5,1},{7,3},{8,12},{10,14},{12... | collective-permute-start | bytes 1419272 | tf_op jit(solution)/shard_map/ppermute | solution.py:347
  103.1 1.3 collective-permute-start.4
  104.4 16.0 %collective-permute-done.4.refs_7_ = bf16[2,2,1408]{2,1,0:T(2,128)(2,1)S(1)} collective-permute-done((bf16[2,2,1408]{2,1,0:T(2,128)(2,1)S(1)}, bf16[2,2,1408]{2,1,0:T(2,128)(2,1)S(1)}, u32[]{:S(2)}, u32[]{:S(2)}) %collective-permute-start.4) | collective-permute-done | bytes 11296 | tf_op jit(solution)/shard_map/ppermute | solution.py:28
  121.5 5.1 %shard_map.111 = (bf16[160,1408]{1,0:T(8,128)(2,1)}, bf16[160,1408]{1,0:T(8,128)(2,1)}, f32[8,1408]{1,0:T(8,128)}) custom-call(bf16[168,1408]{1,0:T(8,128)(2,1)} %copy-done.8, bf16[168,1408]{1,0:T(8,128)(2,1)} %copy-done.9, bf16[168,1408]{1,0:T(8,128)(2,1)} %copy-done.10, bf16[168,1408]{1,0:T(8,128)(2,1)} %copy-done.2, bf16[160,1408]{1,0:T(8,128)(2,1)} %refs_4_.1, ...), custom_call_target="tpu_custom_call" | custom-call | flops 22528000 | bytes 1048576 | tf_op jit(solution)/shard_map/pallas_call | solution.py:269
  126.7 0.8 copy-done.3
  127.4 0.7 shard_map.114
  128.1 11.5 %all_to_all.25.seen_ref = bf16[16,8,384]{2,1,0:T(8,128)(2,1)S(1)} all-to-all(bf16[16,8,384]{2,1,0:T(8,128)(2,1)S(1)} %get-tuple-element.27), channel_id=1, replica_groups=mesh['zh'=4,'zl'=2,'yh'=4,'yl'=2,'fs'=4,'tp'=2] {'zl','yl','fs'}, dimensions={0} | all-to-all | bytes 196608 | tf_op jit(solution)/shard_map/all_to_all | solution.py:32
  139.7 22.3 %all_to_all.26.seen_ref = bf16[16,8,384]{2,1,0:T(8,128)(2,1)S(1)} all-to-all(bf16[16,8,384]{2,1,0:T(8,128)(2,1)S(1)} %shard_map.115), channel_id=1, replica_groups=mesh['zh'=4,'zl'=2,'yh'=4,'yl'=2,'fs'=4,'tp'=2] {'zh','yh'}, dimensions={0} | all-to-all | bytes 196608 | tf_op jit(solution)/shard_map/all_to_all | solution.py:32
  162.0 7.6 %all_to_all.27.seen_ref = f32[4,8,384]{2,1,0:T(8,128)S(1)} all-to-all(f32[4,8,384]{2,1,0:T(8,128)S(1)} %shard_map.116), channel_id=1, replica_groups=mesh['zh'=4,'zl'=2,'yh'=4,'yl'=2,'fs'=4,'tp'=2] {'zl','yl'}, dimensions={0} | all-to-all | bytes 98304 | tf_op jit(solution)/shard_map/all_to_all | solution.py:32
  169.6 0.6 shard_map.117
  170.2 0.6 reduce
  (33 shorter events, 1.5 us)
Async XLA Ops:
  1.5 4.8 %collective-permute-start = (bf16[2,2,1408]{2,1,0:T(2,128)(2,1)S(1)}, bf16[2,2,1408]{2,1,0:T(2,128)(2,1)S(1)}, u32[]{:S(2)}, u32[]{:S(2)}) collective-permute-start(bf16[2,2,1408]{2,1,0:T(2,128)(2,1)S(1)} %pad_maximum_fusion.1), channel_id=1, source_target_pairs={{0,2},{2,4},{4,6},{1,3},{3,5},{5,7},{8,10},{10,12},{12,14},{9,11},... | collective-permute-start | bytes 33800 | tf_op jit(solution)/shard_map/ppermute | solution.py:28
  6.3 0.6 copy-start.11
  11.0 8.5 %copy-start = (bf16[640,512]{1,0:T(8,128)(2,1)S(1)}, bf16[640,512]{1,0:T(8,128)(2,1)}, u32[]{:S(2)}) copy-start(bf16[640,512]{1,0:T(8,128)(2,1)} %own_ref.1) | copy-start | bytes 1966084
  11.1 56.4 %all-to-all-start = ((bf16[16,160,384]{2,1,0:T(8,128)(2,1)}), bf16[16,160,384]{2,1,0:T(8,128)(2,1)S(1)}, u32[]{:S(2)}, u32[]{:S(2)}) async-start(bf16[16,160,384]{2,1,0:T(8,128)(2,1)} %bitcast.23), calls=%async_computation | async-start | bytes 3932160 | tf_op jit(solution)/shard_map/all_to_all | solution.py:32
  19.6 36.6 %collective-permute-start.5 = (bf16[640,512]{1,0:T(8,128)(2,1)S(1)}, bf16[640,512]{1,0:T(8,128)(2,1)S(1)}, u32[]{:S(2)}, u32[]{:S(2)}) collective-permute-start(bf16[640,512]{1,0:T(8,128)(2,1)S(1)} %copy-done), channel_id=1, source_target_pairs={{0,64},{1,9},{8,72},{9,1},{64,0},{65,73},{72,8},{73,65},{2,66},{3,... | collective-permute-start | bytes 1966088 | tf_op jit(solution)/shard_map/ppermute | solution.py:326
  23.0 33.3 %collective-permute-start.6 = (bf16[640,512]{1,0:T(8,128)(2,1)S(1)}, bf16[640,512]{1,0:T(8,128)(2,1)S(1)}, u32[]{:S(2)}, u32[]{:S(2)}) collective-permute-start(bf16[640,512]{1,0:T(8,128)(2,1)S(1)} %copy-done), channel_id=1, source_target_pairs={{0,72},{8,64},{64,8},{72,0},{2,74},{10,66},{66,10},{74,2},{4,76},{... | collective-permute-start | bytes 1966088 | tf_op jit(solution)/shard_map/ppermute | solution.py:327
  56.2 1.3 copy-start.6
  56.2 1.5 copy-start.7
  57.7 5.3 %collective-permute-start.7 = (bf16[2,640,512]{2,1,0:T(8,128)(2,1)}, bf16[2,640,512]{2,1,0:T(8,128)(2,1)}, u32[]{:S(2)}, u32[]{:S(2)}) collective-permute-start(bf16[2,640,512]{2,1,0:T(8,128)(2,1)} %pad_maximum_fusion), channel_id=1, source_target_pairs={{0,1},{1,0},{2,3},{3,2},{4,5},{5,4},{6,7},{7,6},{8,9},{9,8},{10,11... | collective-permute-start | bytes 3932168 | tf_op jit(solution)/shard_map/ppermute | solution.py:328
  67.4 1.3 copy-start.5
  68.7 20.4 %copy-start.1 = (bf16[640,512]{1,0:T(8,128)(2,1)S(1)}, bf16[640,512]{1,0:T(8,128)(2,1)}, u32[]{:S(2)}) copy-start(bf16[640,512]{1,0:T(8,128)(2,1)} %own_ref.1) | copy-start | bytes 1966084
  68.7 20.4 %copy-start.4 = (bf16[1408,512]{1,0:T(8,128)(2,1)S(1)}, bf16[1408,512]{1,0:T(8,128)(2,1)}, u32[]{:S(2)}) copy-start(bf16[1408,512]{1,0:T(8,128)(2,1)} %weight_ref.1) | copy-start | bytes 4325380
  74.1 52.5 %all-to-all-start.1 = ((bf16[64,8,384]{2,1,0:T(8,128)(2,1)}), bf16[64,8,384]{2,1,0:T(8,128)(2,1)S(1)}, u32[]{:S(2)}, u32[]{:S(2)}) async-start(bf16[64,8,384]{2,1,0:T(8,128)(2,1)} %shard_map.113), calls=%async_computation.1 | async-start | bytes 786432 | tf_op jit(solution)/shard_map/all_to_all | solution.py:32
  91.5 0.8 copy-start.2
  92.3 28.1 %collective-permute-start.1 = (bf16[168,1408]{1,0:T(8,128)(2,1)S(1)}, bf16[168,1408]{1,0:T(8,128)(2,1)S(1)}, u32[]{:S(2)}, u32[]{:S(2)}) collective-permute-start(bf16[168,1408]{1,0:T(8,128)(2,1)S(1)} %get-tuple-element.20), channel_id=1, source_target_pairs={{0,2},{2,4},{4,6},{6,0},{1,3},{3,5},{5,7},{7,1},{8,10},{10,12},{12... | collective-permute-start | bytes 1419272 | tf_op jit(solution)/shard_map/ppermute | solution.py:347
  96.1 24.3 %collective-permute-start.2 = (bf16[168,1408]{1,0:T(8,128)(2,1)S(1)}, bf16[168,1408]{1,0:T(8,128)(2,1)S(1)}, u32[]{:S(2)}, u32[]{:S(2)}) collective-permute-start(bf16[168,1408]{1,0:T(8,128)(2,1)S(1)} %get-tuple-element.21), channel_id=1, source_target_pairs={{0,6},{2,0},{4,2},{6,4},{1,7},{3,1},{5,3},{7,5},{8,14},{10,8},{12,... | collective-permute-start | bytes 1419272 | tf_op jit(solution)/shard_map/ppermute | solution.py:347
  99.4 21.0 %collective-permute-start.3 = (bf16[168,1408]{1,0:T(8,128)(2,1)S(1)}, bf16[168,1408]{1,0:T(8,128)(2,1)S(1)}, u32[]{:S(2)}, u32[]{:S(2)}) collective-permute-start(bf16[168,1408]{1,0:T(8,128)(2,1)S(1)} %get-tuple-element.22), channel_id=1, source_target_pairs={{0,4},{2,6},{4,0},{6,2},{1,5},{3,7},{5,1},{7,3},{8,12},{10,14},{12... | collective-permute-start | bytes 1419272 | tf_op jit(solution)/shard_map/ppermute | solution.py:347
  103.1 17.3 %collective-permute-start.4 = (bf16[2,2,1408]{2,1,0:T(2,128)(2,1)S(1)}, bf16[2,2,1408]{2,1,0:T(2,128)(2,1)S(1)}, u32[]{:S(2)}, u32[]{:S(2)}) collective-permute-start(bf16[2,2,1408]{2,1,0:T(2,128)(2,1)S(1)} %pad_maximum_fusion.2), channel_id=1, source_target_pairs={{2,0},{4,2},{6,4},{3,1},{5,3},{7,5},{10,8},{12,10},{14,12},{11,9},... | collective-permute-start | bytes 33800 | tf_op jit(solution)/shard_map/ppermute | solution.py:28
  120.4 0.6 copy-start.12
  120.4 0.8 copy-start.8
  120.4 0.9 copy-start.9
  120.4 1.1 copy-start.10
  126.6 0.8 copy-start.3

commit v3 on v1

--- a/solution.py
+++ b/solution.py
@@ -30,6 +30,22 @@
 
 def swap(array, axes):
     return lax.all_to_all(array, axes, 0, 0, tiled=True)
+
+
+def mate(at, tp):
+    return (at + (1 if (at + tp) % 2 == 0 else -1)) % 8
+
+
+def groups_of(n_fs):
+    groups = []
+    for tp in range(2):
+        for z in range(0, 8, 2):
+            for y in range(0, 8, 2):
+                places = [(i, j) for i in (z, mate(z, tp)) for j in (y, mate(y, tp))]
+                groups.append(
+                    [((i * 8 + j) * n_fs + x) * 2 + tp for i, j in places for x in range(n_fs)]
+                )
+    return groups
 
 
 def call(body, out_shape, flops=0, limit=8, **kw):
@@ -111,36 +127,43 @@
     )(at, cotangent, weight)
 
 
-def grad_body(order_ref, own, side, far, across, hidden, out_ref, cot_ref, rows_ref, cot_sem, row_sem):
-    tokens = own.shape[0]
-    core = order_ref[GROUP]
-
-    def fetch(k, source):
-        spot = pl.ds(k * tokens, tokens)
-        return pltpu.make_async_copy(source, cot_ref.at[spot], cot_sem.at[k])
+def order_body(order_ref, out_ref):
+    for k in range(GROUP):
+        out_ref[k] = order_ref[k]
+
+
+def order_of(order):
+    scalars = pl.BlockSpec(memory_space=pltpu.SMEM)
+    return call(
+        order_body,
+        jax.ShapeDtypeStruct(order.shape, order.dtype),
+        in_specs=[scalars],
+        out_specs=scalars,
+    )(order)
+
+
+def grad_body(order_ref, *refs):
+    blocks, hidden = refs[:GROUP], refs[GROUP]
+    out_ref, cot_ref, rows_ref, cot_sem, row_sem = refs[GROUP + 1 :]
+    tokens = hidden.shape[1]
+
+    def fetch(k):
+        return pltpu.make_async_copy(
+            blocks[k], cot_ref.at[pl.ds(k * tokens, tokens)], cot_sem.at[k]
+        )
 
     def fetch_rows(k):
-        spot = pl.ds(k * tokens, tokens)
-        return pltpu.make_async_copy(hidden.at[order_ref[k]], rows_ref.at[spot], row_sem.at[k])
-
-    blocks = [fetch(0, own), fetch(1, side), fetch(2, across.at[0])]
-    for k, copy in enumerate(blocks):
-        copy.start()
+        return pltpu.make_async_copy(
+            hidden.at[order_ref[k]], rows_ref.at[pl.ds(k * tokens, tokens)], row_sem.at[k]
+        )
+
+    for k in range(GROUP):
+        fetch(k).start()
         fetch_rows(k).start()
-
-    @pl.when(core == 0)
-    def _():
-        fetch(3, far).start()
-
-    @pl.when(core != 0)
-    def _():
-        fetch(3, across.at[1]).start()
-
-    fetch_rows(3).start()
     total = None
     for part in range(2):
         for k in (2 * part, 2 * part + 1):
-            fetch(k, own).wait()
+            fetch(k).wait()
             fetch_rows(k).wait()
         span = slice(2 * part * tokens, 2 * (part + 1) * tokens)
         value = lax.dot_general(
@@ -150,15 +173,16 @@
     out_ref[...] = total.astype(BF16).reshape(out_ref.shape)
 
 
-def grad_of(order, own, side, far, across, hidden, n_rep):
-    tokens, depth = own.shape
+def grad_of(order, blocks, hidden, n_rep):
+    tokens, depth = blocks[0].shape
     block = hidden.shape[2]
     return call(
         grad_body,
         jax.ShapeDtypeStruct((n_rep, depth // n_rep, block), BF16),
         flops=2 * GROUP * tokens * depth * block,
         limit=60,
-        in_specs=[pl.BlockSpec(memory_space=pltpu.SMEM)] + [pl.BlockSpec(memory_space=pl.ANY)] * 5,
+        in_specs=[pl.BlockSpec(memory_space=pltpu.SMEM)]
+        + [pl.BlockSpec(memory_space=pl.ANY)] * (GROUP + 1),
         out_specs=pl.BlockSpec(memory_space=pltpu.VMEM),
         scratch_shapes=[
             pltpu.VMEM((GROUP * tokens, depth), BF16),
@@ -166,7 +190,7 @@
             pltpu.SemaphoreType.DMA((GROUP,)),
             pltpu.SemaphoreType.DMA((GROUP,)),
         ],
-    )(order, own, side, far, across, hidden)
+    )(order, *blocks, hidden)
 
 
 def share_body(scale, parts_ref, taps_ref, grad_ref, small_ref):
@@ -296,24 +320,31 @@
     before = passed_along(jnp.stack([gate_pre[-HALO:], up_pre[-HALO:]]), "fs", 1)
     after = passed_along(jnp.stack([gate_pre[:HALO], up_pre[:HALO]]), "fs", -1)
 
-    axes = ("zl", "yl", "tp")
-    first, second = [], []
-    for i in range(8):
-        flip = 4 if i % 2 == 0 else 2
-        first.append((i, i ^ flip))
-        if i % 2 == 0:
-            second.append((i, i ^ 6))
-    side = lax.ppermute(cotangent, axes, first)
-    far = lax.ppermute(cotangent, axes, second)
-    across = lax.ppermute(jnp.stack([side, far]), "tp", [(0, 1), (1, 0)])
-    tp = lax.axis_index("tp")
+    def collected(flip_z, flip_y):
+        pairs = []
+        for z in range(8):
+            for y in range(8):
+                for tp in range(2):
+                    to_z = mate(z, tp) if flip_z else z
+                    to_y = mate(y, tp) if flip_y else y
+                    pairs.append(((z * 8 + y) * 2 + tp, (to_z * 8 + to_y) * 2 + tp))
+        return lax.ppermute(cotangent, ZY + ("tp",), pairs)
+
+    blocks = [cotangent, collected(True, False)]
+    blocks.append(collected(False, True))
+    blocks.append(collected(True, True))
     member = lax.axis_index("zl") * 2 + lax.axis_index("yl")
-    order = jnp.stack(
-        [member, member ^ (2 - tp), member ^ (1 + tp), member ^ 3, tp]
+    order = order_of(jnp.stack([member, member ^ 2, member ^ 1, member ^ 3]))
+
+    hidden = hidden_of(gate_pre, up_pre, before, gate_taps, up_taps, block, n_fs)
+    everyone = lax.all_to_all(
+        hidden.reshape(n_near, rows, block),
+        TOK + ("tp",),
+        0,
+        0,
+        tiled=True,
+        axis_index_groups=groups_of(n_fs),
     )
-
-    hidden = hidden_of(gate_pre, up_pre, before, gate_taps, up_taps, block, n_fs)
-    everyone = swap(hidden.reshape(n_near, rows, block), NEAR)
 
     me = lax.axis_index("fs")
     steps = (1, 3, 2, 0)
@@ -324,9 +355,7 @@
         pairs = [(i, (i + step) % n_fs) for i in range(n_fs)]
         terms[k] = lax.ppermute(terms[k], "fs", pairs)
 
-    partial = grad_of(
-        order, cotangent, side, far, across, everyone.reshape(GROUP, -1, block), n_rep
-    )
+    partial = grad_of(order, blocks, everyone.reshape(GROUP, -1, block), n_rep)
     parts = swap(partial, ZY)
 
     grad_gate, grad_up, taps = chain_of(

time: 167 us -> 155 us (0.928)
  waiting for transfers between devices: 51.4 us -> 35.1 us
  starting transfers between devices: 46.1 us -> 49.8 us
    ppermute x3, waiting for transfers between devices: 34 us -> 21.8 us  [collected(): return lax.ppermute(cotangent, ZY + ('tp',), pairs)]
    all_to_all x0 -> x1, starting transfers between devices: none -> 8.51 us  [local(): lax.all_to_all(hidden.reshape(n_near, rows, block), TOK + ('tp',), 0, 0,...]
    all_to_all x2 -> x1, starting transfers between devices: 23.4 us -> 17.6 us  [swap(): return lax.all_to_all(array, axes, 0, 0, tiled=True)]
    ppermute x2, waiting for transfers between devices: 17.4 us -> 13.3 us  [passed_along(): return lax.ppermute(array, axis, pairs)]
    ppermute x3, starting transfers between devices: 7.29 us -> 9.22 us  [collected(): return lax.ppermute(cotangent, ZY + ('tp',), pairs)]
    unnamed x26 -> x24, local copies, waits for them, and re-layouts: 4.72 us -> 5.05 us
  transfers between devices with their start and end apart: 10 -> 10, of which waited for: 4 -> 4; matrix products, arithmetic and copies ran while one was open for 1% -> 0% of each run, Pallas kernels for 5% -> 6%
where the time goes in v3:
time: 155 us; the launch traced here: 154 us
  starting transfers between devices  49.8 us (32%)
  blocking collectives  41.8 us (27%)
  waiting for transfers between devices  35.1 us (23%)
  Pallas kernels  19.7 us (13%)
  local copies, waits for them, and re-layouts  5.86 us (4%)
    all_to_all x3, blocking collectives, swap(): return lax.all_to_all(array, axes, 0, 0, tiled=True)  41.8 us
    ppermute x3, waiting for transfers between devices, collected(): return lax.ppermute(cotangent, ZY + ('tp',), pairs)  21.8 us
    all_to_all x1, starting transfers between devices, swap(): return lax.all_to_all(array, axes, 0, 0, tiled=True)  17.6 us
    ppermute x2, waiting for transfers between devices, passed_along(): return lax.ppermute(array, axis, pairs)  13.3 us
    ppermute x3, starting transfers between devices, local(): terms[k] = lax.ppermute(terms[k], 'fs', pairs)  9.81 us
    ppermute x3, starting transfers between devices, collected(): return lax.ppermute(cotangent, ZY + ('tp',), pairs)  9.22 us
    all_to_all x1, starting transfers between devices, local(): lax.all_to_all(hidden.reshape(n_near, rows, block), TOK + ('tp',), 0, 0,...  8.51 us
    pallas_call x1, Pallas kernels, grad_of(): call(grad_body, jax.ShapeDtypeStruct((n_rep, depth // n_rep, block), BF16...  5.42 us
  transfers between devices with their start and end apart: 10, of which 4 were waited for; matrix products, arithmetic and copies ran while one was open for 0% of the time, Pallas kernels for 6%

profile of v3, /device:TPU:8, one launch (start us, length us, event | category | flops | bytes accessed | tf_op | source)
XLA Modules:
  0.0 154.0 jit_solution(6690940280453112366)
XLA Ops:
  0.6 0.8 slice_bitcast_fusion
  1.5 3.4 %collective-permute-start = (bf16[2,2,1408]{2,1,0:T(2,128)(2,1)S(1)}, bf16[2,2,1408]{2,1,0:T(2,128)(2,1)S(1)}, u32[]{:S(2)}, u32[]{:S(2)}) collective-permute-start(bf16[2,2,1408]{2,1,0:T(2,128)(2,1)S(1)} %pad_maximum_fusion), channel_id=1, source_target_pairs={{0,2},{2,4},{4,6},{1,3},{3,5},{5,7},{8,10},{10,12},{12,14},{9,11},... | collective-permute-start | bytes 33800 | tf_op jit(solution)/shard_map/ppermute | solution.py:28
  4.9 1.4 collective-permute-done.before_ref.refs_6_
  6.3 0.6 copy-done.10
  6.9 4.2 %shard_map.109 = bf16[4,4,160,384]{3,2,1,0:T(8,128)(2,1)} custom-call(bf16[160,1408]{1,0:T(8,128)(2,1)} %refs_4_.1, bf16[160,1408]{1,0:T(8,128)(2,1)} %refs_5_.1, bf16[2,2,1408]{2,1,0:T(2,128)(2,1)} %copy-done.10, bf16[3,1408]{1,0:T(4,128)(2,1)} %refs_8_.1, bf16[3,1408]{1,0:T(4,128)(2,1)} %refs_9_.1), custom_call_target="tpu_custom_call" | custom-call | flops 9011200 | bytes 1048576 | tf_op jit(solution)/shard_map/pallas_call | solution.py:87
  11.1 8.5 %all-to-all-start = ((bf16[16,160,384]{2,1,0:T(8,128)(2,1)}), bf16[16,160,384]{2,1,0:T(8,128)(2,1)S(1)}, u32[]{:S(2)}, u32[]{:S(2)}) async-start(bf16[16,160,384]{2,1,0:T(8,128)(2,1)} %bitcast.20), calls=%async_computation | async-start | bytes 3932160 | tf_op jit(solution)/shard_map/all_to_all | solution.py:340
  19.6 3.4 %collective-permute-start.5 = (bf16[640,512]{1,0:T(8,128)(2,1)S(1)}, bf16[640,512]{1,0:T(8,128)(2,1)}, u32[]{:S(2)}, u32[]{:S(2)}) collective-permute-start(bf16[640,512]{1,0:T(8,128)(2,1)S(1)} %copy-done), channel_id=1, source_target_pairs={{0,64},{1,449},{8,72},{9,457},{16,80},{17,465},{24,88},{25,473},{3... | collective-permute-start | bytes 1966088 | tf_op jit(solution)/shard_map/ppermute | solution.py:331
  23.0 2.5 %collective-permute-start.6 = (bf16[640,512]{1,0:T(8,128)(2,1)S(1)}, bf16[640,512]{1,0:T(8,128)(2,1)}, u32[]{:S(2)}, u32[]{:S(2)}) collective-permute-start(bf16[640,512]{1,0:T(8,128)(2,1)S(1)} %copy-done), channel_id=1, source_target_pairs={{0,8},{1,57},{8,0},{9,17},{16,24},{17,9},{24,16},{25,33},{32,40},{... | collective-permute-start | bytes 1966088 | tf_op jit(solution)/shard_map/ppermute | solution.py:331
  25.5 3.4 %collective-permute-start.7 = (bf16[640,512]{1,0:T(8,128)(2,1)S(1)}, bf16[640,512]{1,0:T(8,128)(2,1)}, u32[]{:S(2)}, u32[]{:S(2)}) collective-permute-start(bf16[640,512]{1,0:T(8,128)(2,1)S(1)} %copy-done), channel_id=1, source_target_pairs={{0,72},{1,505},{8,64},{9,465},{16,88},{17,457},{24,80},{25,481},{3... | collective-permute-start | bytes 1966088 | tf_op jit(solution)/shard_map/ppermute | solution.py:331
  28.9 1.1 shard_map.112.order_ref
  30.1 0.5 copy-done.4
  30.6 21.5 %collective-permute-done.5.refs_1_ = bf16[640,512]{1,0:T(8,128)(2,1)} collective-permute-done((bf16[640,512]{1,0:T(8,128)(2,1)S(1)}, bf16[640,512]{1,0:T(8,128)(2,1)}, u32[]{:S(2)}, u32[]{:S(2)}) %collective-permute-start.5) | collective-permute-done | bytes 655392 | tf_op jit(solution)/shard_map/ppermute | solution.py:331
  52.1 0.3 collective-permute-done.7.refs_3_
  52.4 1.3 copy-done.6
  53.7 5.4 %shard_map.113 = bf16[64,8,384]{2,1,0:T(8,128)(2,1)} custom-call(s32[4]{0:T(128)} %copy-done.4, bf16[640,512]{1,0:T(8,128)(2,1)} %refs_0_.1, bf16[640,512]{1,0:T(8,128)(2,1)} %collective-permute-done.5.refs_1_, bf16[640,512]{1,0:T(8,128)(2,1)} %collective-permute-done.6.refs_2_, bf16[640,512]{1,0:T(8,128)(2,1)} %collective-permute-done.7.refs_3_, ...), custom_call_target="tpu_custom_call" | custom-call | flops 1006632960 | bytes 1048576 | tf_op jit(solution)/shard_map/pallas_call | solution.py:179
  59.1 17.6 %all-to-all-start.1 = ((bf16[64,8,384]{2,1,0:T(8,128)(2,1)}), bf16[64,8,384]{2,1,0:T(8,128)(2,1)S(1)}, u32[]{:S(2)}, u32[]{:S(2)}) async-start(bf16[64,8,384]{2,1,0:T(8,128)(2,1)} %shard_map.113), calls=%async_computation.1 | async-start | bytes 786432 | tf_op jit(solution)/shard_map/all_to_all | solution.py:32
  76.8 2.4 %shard_map.110 = (bf16[168,1408]{1,0:T(8,128)(2,1)S(1)}, bf16[168,1408]{1,0:T(8,128)(2,1)S(1)}, bf16[168,1408]{1,0:T(8,128)(2,1)S(1)}, bf16[168,1408]{1,0:T(8,128)(2,1)S(1)}) custom-call(s32[4]{0:T(128)S(1)} %pad_add_fusion.at_ref, bf16[640,512]{1,0:T(8,128)(2,1)S(1)} %copy-done.1, bf16[1408,512]{1,0:T(8,128)(2,1)S(1)} %copy-done.5), custom_call_target="tpu_custom_call" | custom-call | flops 922746880 | bytes 1048576 | tf_op jit(solution)/shard_map/pallas_call | solution.py:119
  79.3 0.8 copy-done.2
  80.0 3.5 %collective-permute-start.1 = (bf16[168,1408]{1,0:T(8,128)(2,1)S(1)}, bf16[168,1408]{1,0:T(8,128)(2,1)S(1)}, u32[]{:S(2)}, u32[]{:S(2)}) collective-permute-start(bf16[168,1408]{1,0:T(8,128)(2,1)S(1)} %get-tuple-element.20), channel_id=1, source_target_pairs={{0,2},{2,4},{4,6},{6,0},{1,3},{3,5},{5,7},{7,1},{8,10},{10,12},{12... | collective-permute-start | bytes 1419272 | tf_op jit(solution)/shard_map/ppermute | solution.py:356
  83.5 3.6 %collective-permute-start.2 = (bf16[168,1408]{1,0:T(8,128)(2,1)S(1)}, bf16[168,1408]{1,0:T(8,128)(2,1)S(1)}, u32[]{:S(2)}, u32[]{:S(2)}) collective-permute-start(bf16[168,1408]{1,0:T(8,128)(2,1)S(1)} %get-tuple-element.21), channel_id=1, source_target_pairs={{0,6},{2,0},{4,2},{6,4},{1,7},{3,1},{5,3},{7,5},{8,14},{10,8},{12,... | collective-permute-start | bytes 1419272 | tf_op jit(solution)/shard_map/ppermute | solution.py:356
  87.1 2.8 %collective-permute-start.3 = (bf16[168,1408]{1,0:T(8,128)(2,1)S(1)}, bf16[168,1408]{1,0:T(8,128)(2,1)S(1)}, u32[]{:S(2)}, u32[]{:S(2)}) collective-permute-start(bf16[168,1408]{1,0:T(8,128)(2,1)S(1)} %get-tuple-element.22), channel_id=1, source_target_pairs={{0,4},{2,6},{4,0},{6,2},{1,5},{3,7},{5,1},{7,3},{8,12},{10,14},{12... | collective-permute-start | bytes 1419272 | tf_op jit(solution)/shard_map/ppermute | solution.py:356
  89.9 1.3 collective-permute-start.4
  91.2 11.9 %collective-permute-done.4.refs_7_ = bf16[2,2,1408]{2,1,0:T(2,128)(2,1)S(1)} collective-permute-done((bf16[2,2,1408]{2,1,0:T(2,128)(2,1)S(1)}, bf16[2,2,1408]{2,1,0:T(2,128)(2,1)S(1)}, u32[]{:S(2)}, u32[]{:S(2)}) %collective-permute-start.4) | collective-permute-done | bytes 11296 | tf_op jit(solution)/shard_map/ppermute | solution.py:28
  103.2 0.6 copy-done.11
  104.2 5.1 %shard_map.111 = (bf16[160,1408]{1,0:T(8,128)(2,1)}, bf16[160,1408]{1,0:T(8,128)(2,1)}, f32[8,1408]{1,0:T(8,128)}) custom-call(bf16[168,1408]{1,0:T(8,128)(2,1)} %copy-done.7, bf16[168,1408]{1,0:T(8,128)(2,1)} %copy-done.8, bf16[168,1408]{1,0:T(8,128)(2,1)} %copy-done.9, bf16[168,1408]{1,0:T(8,128)(2,1)} %copy-done.2, bf16[160,1408]{1,0:T(8,128)(2,1)} %refs_4_.1, ...), custom_call_target="tpu_custom_call" | custom-call | flops 22528000 | bytes 1048576 | tf_op jit(solution)/shard_map/pallas_call | solution.py:273
  109.4 0.8 copy-done.3
  110.2 0.7 shard_map.114
  110.9 11.9 %all_to_all.25.seen_ref = bf16[16,8,384]{2,1,0:T(8,128)(2,1)S(1)} all-to-all(bf16[16,8,384]{2,1,0:T(8,128)(2,1)S(1)} %get-tuple-element.27), channel_id=1, replica_groups=mesh['zh'=4,'zl'=2,'yh'=4,'yl'=2,'fs'=4,'tp'=2] {'zl','yl','fs'}, dimensions={0} | all-to-all | bytes 196608 | tf_op jit(solution)/shard_map/all_to_all | solution.py:32
  122.8 22.2 %all_to_all.26.seen_ref = bf16[16,8,384]{2,1,0:T(8,128)(2,1)S(1)} all-to-all(bf16[16,8,384]{2,1,0:T(8,128)(2,1)S(1)} %shard_map.115), channel_id=1, replica_groups=mesh['zh'=4,'zl'=2,'yh'=4,'yl'=2,'fs'=4,'tp'=2] {'zh','yh'}, dimensions={0} | all-to-all | bytes 196608 | tf_op jit(solution)/shard_map/all_to_all | solution.py:32
  145.1 7.6 %all_to_all.27.seen_ref = f32[4,8,384]{2,1,0:T(8,128)S(1)} all-to-all(f32[4,8,384]{2,1,0:T(8,128)S(1)} %shard_map.116), channel_id=1, replica_groups=mesh['zh'=4,'zl'=2,'yh'=4,'yl'=2,'fs'=4,'tp'=2] {'zl','yl'}, dimensions={0} | all-to-all | bytes 98304 | tf_op jit(solution)/shard_map/all_to_all | solution.py:32
  152.7 0.6 shard_map.117
  153.3 0.6 reduce
  (30 shorter events, 0.8 us)
Async XLA Ops:
  1.5 4.8 %collective-permute-start = (bf16[2,2,1408]{2,1,0:T(2,128)(2,1)S(1)}, bf16[2,2,1408]{2,1,0:T(2,128)(2,1)S(1)}, u32[]{:S(2)}, u32[]{:S(2)}) collective-permute-start(bf16[2,2,1408]{2,1,0:T(2,128)(2,1)S(1)} %pad_maximum_fusion), channel_id=1, source_target_pairs={{0,2},{2,4},{4,6},{1,3},{3,5},{5,7},{8,10},{10,12},{12,14},{9,11},... | collective-permute-start | bytes 33800 | tf_op jit(solution)/shard_map/ppermute | solution.py:28
  6.3 0.6 copy-start.10
  11.1 8.5 %copy-start = (bf16[640,512]{1,0:T(8,128)(2,1)S(1)}, bf16[640,512]{1,0:T(8,128)(2,1)}, u32[]{:S(2)}) copy-start(bf16[640,512]{1,0:T(8,128)(2,1)} %refs_0_.1) | copy-start | bytes 1966084
  11.1 41.3 %all-to-all-start = ((bf16[16,160,384]{2,1,0:T(8,128)(2,1)}), bf16[16,160,384]{2,1,0:T(8,128)(2,1)S(1)}, u32[]{:S(2)}, u32[]{:S(2)}) async-start(bf16[16,160,384]{2,1,0:T(8,128)(2,1)} %bitcast.20), calls=%async_computation | async-start | bytes 3932160 | tf_op jit(solution)/shard_map/all_to_all | solution.py:340
  19.6 32.5 %collective-permute-start.5 = (bf16[640,512]{1,0:T(8,128)(2,1)S(1)}, bf16[640,512]{1,0:T(8,128)(2,1)}, u32[]{:S(2)}, u32[]{:S(2)}) collective-permute-start(bf16[640,512]{1,0:T(8,128)(2,1)S(1)} %copy-done), channel_id=1, source_target_pairs={{0,64},{1,449},{8,72},{9,457},{16,80},{17,465},{24,88},{25,473},{3... | collective-permute-start | bytes 1966088 | tf_op jit(solution)/shard_map/ppermute | solution.py:331
  23.0 29.1 %collective-permute-start.6 = (bf16[640,512]{1,0:T(8,128)(2,1)S(1)}, bf16[640,512]{1,0:T(8,128)(2,1)}, u32[]{:S(2)}, u32[]{:S(2)}) collective-permute-start(bf16[640,512]{1,0:T(8,128)(2,1)S(1)} %copy-done), channel_id=1, source_target_pairs={{0,8},{1,57},{8,0},{9,17},{16,24},{17,9},{24,16},{25,33},{32,40},{... | collective-permute-start | bytes 1966088 | tf_op jit(solution)/shard_map/ppermute | solution.py:331
  25.5 26.9 %collective-permute-start.7 = (bf16[640,512]{1,0:T(8,128)(2,1)S(1)}, bf16[640,512]{1,0:T(8,128)(2,1)}, u32[]{:S(2)}, u32[]{:S(2)}) collective-permute-start(bf16[640,512]{1,0:T(8,128)(2,1)S(1)} %copy-done), channel_id=1, source_target_pairs={{0,72},{1,505},{8,64},{9,465},{16,88},{17,457},{24,80},{25,481},{3... | collective-permute-start | bytes 1966088 | tf_op jit(solution)/shard_map/ppermute | solution.py:331
  30.1 0.5 copy-start.4
  52.4 1.3 copy-start.6
  53.7 23.2 %copy-start.1 = (bf16[640,512]{1,0:T(8,128)(2,1)S(1)}, bf16[640,512]{1,0:T(8,128)(2,1)}, u32[]{:S(2)}) copy-start(bf16[640,512]{1,0:T(8,128)(2,1)} %refs_0_.1) | copy-start | bytes 1966084
  53.7 23.2 %copy-start.5 = (bf16[1408,512]{1,0:T(8,128)(2,1)S(1)}, bf16[1408,512]{1,0:T(8,128)(2,1)}, u32[]{:S(2)}) copy-start(bf16[1408,512]{1,0:T(8,128)(2,1)} %weight_ref.1) | copy-start | bytes 4325380
  59.1 50.3 %all-to-all-start.1 = ((bf16[64,8,384]{2,1,0:T(8,128)(2,1)}), bf16[64,8,384]{2,1,0:T(8,128)(2,1)S(1)}, u32[]{:S(2)}, u32[]{:S(2)}) async-start(bf16[64,8,384]{2,1,0:T(8,128)(2,1)} %shard_map.113), calls=%async_computation.1 | async-start | bytes 786432 | tf_op jit(solution)/shard_map/all_to_all | solution.py:32
  79.3 0.8 copy-start.2
  80.0 23.1 %collective-permute-start.1 = (bf16[168,1408]{1,0:T(8,128)(2,1)S(1)}, bf16[168,1408]{1,0:T(8,128)(2,1)S(1)}, u32[]{:S(2)}, u32[]{:S(2)}) collective-permute-start(bf16[168,1408]{1,0:T(8,128)(2,1)S(1)} %get-tuple-element.20), channel_id=1, source_target_pairs={{0,2},{2,4},{4,6},{6,0},{1,3},{3,5},{5,7},{7,1},{8,10},{10,12},{12... | collective-permute-start | bytes 1419272 | tf_op jit(solution)/shard_map/ppermute | solution.py:356
  83.5 19.6 %collective-permute-start.2 = (bf16[168,1408]{1,0:T(8,128)(2,1)S(1)}, bf16[168,1408]{1,0:T(8,128)(2,1)S(1)}, u32[]{:S(2)}, u32[]{:S(2)}) collective-permute-start(bf16[168,1408]{1,0:T(8,128)(2,1)S(1)} %get-tuple-element.21), channel_id=1, source_target_pairs={{0,6},{2,0},{4,2},{6,4},{1,7},{3,1},{5,3},{7,5},{8,14},{10,8},{12,... | collective-permute-start | bytes 1419272 | tf_op jit(solution)/shard_map/ppermute | solution.py:356
  87.1 16.1 %collective-permute-start.3 = (bf16[168,1408]{1,0:T(8,128)(2,1)S(1)}, bf16[168,1408]{1,0:T(8,128)(2,1)S(1)}, u32[]{:S(2)}, u32[]{:S(2)}) collective-permute-start(bf16[168,1408]{1,0:T(8,128)(2,1)S(1)} %get-tuple-element.22), channel_id=1, source_target_pairs={{0,4},{2,6},{4,0},{6,2},{1,5},{3,7},{5,1},{7,3},{8,12},{10,14},{12... | collective-permute-start | bytes 1419272 | tf_op jit(solution)/shard_map/ppermute | solution.py:356
  89.9 13.2 %collective-permute-start.4 = (bf16[2,2,1408]{2,1,0:T(2,128)(2,1)S(1)}, bf16[2,2,1408]{2,1,0:T(2,128)(2,1)S(1)}, u32[]{:S(2)}, u32[]{:S(2)}) collective-permute-start(bf16[2,2,1408]{2,1,0:T(2,128)(2,1)S(1)} %pad_maximum_fusion.1), channel_id=1, source_target_pairs={{2,0},{4,2},{6,4},{3,1},{5,3},{7,5},{10,8},{12,10},{14,12},{11,9},... | collective-permute-start | bytes 33800 | tf_op jit(solution)/shard_map/ppermute | solution.py:28
  103.1 0.6 copy-start.11
  103.1 0.8 copy-start.7
  103.1 0.9 copy-start.8
  103.2 1.1 copy-start.9
  109.4 0.8 copy-start.3

commit v4 on v3

--- a/solution.py
+++ b/solution.py
@@ -62,22 +62,23 @@
     step = pl.program_id(0)
     block = gate_ref.shape[1]
 
-    def conv(which, source, taps):
-        held_ref[PAD - HALO : PAD] = before_ref[which].astype(F32)
-        held_ref[PAD : PAD + rows] = source[...].astype(F32)
-        total = taps[2:3].astype(F32) * held_ref[PAD : PAD + rows]
+    def conv(which, source, taps, lanes):
+        held_ref[which, PAD - HALO : PAD] = before_ref[which, :, lanes].astype(F32)
+        held_ref[which, PAD : PAD + rows] = source[:, lanes].astype(F32)
+        total = taps[2:3, lanes].astype(F32) * held_ref[which, PAD : PAD + rows]
         for k in range(2):
             start = PAD - HALO + k
-            total += taps[k : k + 1].astype(F32) * held_ref[start : start + rows]
+            total += taps[k : k + 1, lanes].astype(F32) * held_ref[which, start : start + rows]
         return total
 
-    gate = conv(0, gate_ref, gate_taps)
-    up = conv(1, up_ref, up_taps)
-    value = gate * (1.0 / (1.0 + jnp.exp(-gate))) * up
-    lane = lax.broadcasted_iota(jnp.int32, value.shape, 1) + step * block
-    value = jnp.where(lane < width, value, 0.0).astype(BF16)
-    for k in range(out_ref.shape[1]):
-        out_ref[0, k] = value
+    for at in range(0, block, LANE):
+        lanes = slice(at, at + LANE)
+        gate = conv(0, gate_ref, gate_taps, lanes)
+        up = conv(1, up_ref, up_taps, lanes)
+        value = gate * (1.0 / (1.0 + jnp.exp(-gate))) * up
+        value = jnp.where(step * block + at < width, value, 0.0).astype(BF16)
+        for k in range(out_ref.shape[1]):
+            out_ref[0, k, :, lanes] = value
 
 
 def hidden_of(gate_pre, up_pre, before, gate_taps, up_taps, block, n_fs):
@@ -88,11 +89,11 @@
         functools.partial(hidden_body, rows, width),
         jax.ShapeDtypeStruct((GROUP, n_fs, rows, block), BF16),
         flops=40 * rows * width,
-        limit=60,
+        limit=62,
         grid=(GROUP,),
         in_specs=[wide, wide, pl.BlockSpec((2, HALO, block), lambda i: (0, 0, i)), taps, taps],
         out_specs=pl.BlockSpec((1, n_fs, rows, block), lambda i: (i, 0, 0, 0)),
-        scratch_shapes=[pltpu.VMEM((rows + PAD, block), F32)],
+        scratch_shapes=[pltpu.VMEM((2, rows + PAD, LANE), F32)],
     )(gate_pre, up_pre, before, gate_taps, up_taps)
 
 
@@ -161,11 +162,10 @@
         fetch(k).start()
         fetch_rows(k).start()
     total = None
-    for part in range(2):
-        for k in (2 * part, 2 * part + 1):
-            fetch(k).wait()
-            fetch_rows(k).wait()
-        span = slice(2 * part * tokens, 2 * (part + 1) * tokens)
+    for k in range(GROUP):
+        fetch(k).wait()
+        fetch_rows(k).wait()
+        span = slice(k * tokens, (k + 1) * tokens)
         value = lax.dot_general(
             cot_ref[span], rows_ref[span], (((0,), (0,)), ((), ())), preferred_element_type=F32
         )
@@ -180,7 +180,7 @@
         grad_body,
         jax.ShapeDtypeStruct((n_rep, depth // n_rep, block), BF16),
         flops=2 * GROUP * tokens * depth * block,
-        limit=60,
+        limit=62,
         in_specs=[pl.BlockSpec(memory_space=pltpu.SMEM)]
         + [pl.BlockSpec(memory_space=pl.ANY)] * (GROUP + 1),
         out_specs=pl.BlockSpec(memory_space=pltpu.VMEM),
@@ -274,7 +274,7 @@
         functools.partial(chain_body, rows),
         (grad, grad, jax.ShapeDtypeStruct((8, width), F32)),
         flops=100 * rows * width,
-        limit=60,
+        limit=62,
         grid=(GROUP,),
         in_specs=[tall] * 4 + [wide, wide, edge, edge, taps, taps],
         out_specs=(wide, wide, pl.BlockSpec((8, block), lambda i: (0, i))),
@@ -305,7 +305,7 @@
         lanes = slice(start, start + size)
         gate_ref[:, lanes] = seen_ref[member, :3, :size] * scale
         up_ref[:, lanes] = seen_ref[member, 3:6, :size] * scale
-        norm_ref[:, lanes] = seen_ref[member, 7:, :size] / D
+        norm_ref[lanes] = seen_ref[member, 7, :size] / D
 
 
 def local(gate_pre, up_pre, gate_taps, up_taps, down_weight, cotangent):
@@ -371,9 +371,9 @@
     three = jax.ShapeDtypeStruct((3, width), F32)
     gate_out, up_out, norms = call(
         functools.partial(last_body, grad_scale),
-        (three, three, jax.ShapeDtypeStruct((1, width), F32)),
+        (three, three, jax.ShapeDtypeStruct((width,), F32)),
     )(swap(small, ("zl", "yl")))
-    return grad_gate, grad_up, gate_out, up_out, grad_share[None], norms[0]
+    return grad_gate, grad_up, gate_out, up_out, grad_share[None], norms
 
 
 def solution(mesh):

time: 155 us -> 155 us (level)
    unnamed x24 -> x28, local copies, waits for them, and re-layouts: 5.05 us -> 6.17 us
where the time goes in v4:
time: 155 us; the launch traced here: 154 us
  starting transfers between devices  49.6 us (32%)
  blocking collectives  41.7 us (27%)
  waiting for transfers between devices  35.4 us (23%)
  Pallas kernels  19.5 us (13%)
  local copies, waits for them, and re-layouts  6.98 us (5%)
    all_to_all x3, blocking collectives, swap(): return lax.all_to_all(array, axes, 0, 0, tiled=True)  41.7 us
    ppermute x3, waiting for transfers between devices, collected(): return lax.ppermute(cotangent, ZY + ('tp',), pairs)  21.7 us
    all_to_all x1, starting transfers between devices, swap(): return lax.all_to_all(array, axes, 0, 0, tiled=True)  17.8 us
    ppermute x2, waiting for transfers between devices, passed_along(): return lax.ppermute(array, axis, pairs)  13.7 us
    ppermute x3, starting transfers between devices, local(): terms[k] = lax.ppermute(terms[k], 'fs', pairs)  9.41 us
    ppermute x3, starting transfers between devices, collected(): return lax.ppermute(cotangent, ZY + ('tp',), pairs)  9.21 us
    all_to_all x1, starting transfers between devices, local(): lax.all_to_all(hidden.reshape(n_near, rows, block), TOK + ('tp',), 0, 0,...  8.51 us
    unnamed x28, local copies, waits for them, and re-layouts  6.17 us
  transfers between devices with their start and end apart: 10, of which 4 were waited for; matrix products, arithmetic and copies ran while one was open for 0% of the time, Pallas kernels for 6%

profile of v4, /device:TPU:8, one launch (start us, length us, event | category | flops | bytes accessed | tf_op | source)
XLA Modules:
  0.0 154.3 jit_solution(16407761230524227463)
XLA Ops:
  0.6 0.8 slice_bitcast_fusion
  1.5 3.4 %collective-permute-start = (bf16[2,2,1408]{2,1,0:T(2,128)(2,1)S(1)}, bf16[2,2,1408]{2,1,0:T(2,128)(2,1)S(1)}, u32[]{:S(2)}, u32[]{:S(2)}) collective-permute-start(bf16[2,2,1408]{2,1,0:T(2,128)(2,1)S(1)} %pad_maximum_fusion), channel_id=1, source_target_pairs={{0,2},{2,4},{4,6},{1,3},{3,5},{5,7},{8,10},{10,12},{12,14},{9,11},... | collective-permute-start | bytes 33800 | tf_op jit(solution)/shard_map/ppermute | solution.py:28
  4.9 1.4 collective-permute-done.before_ref.refs_6_
  6.3 0.6 copy-done.12
  6.9 3.9 %shard_map.109 = bf16[4,4,160,384]{3,2,1,0:T(8,128)(2,1)} custom-call(bf16[160,1408]{1,0:T(8,128)(2,1)} %refs_4_.1, bf16[160,1408]{1,0:T(8,128)(2,1)} %refs_5_.1, bf16[2,2,1408]{2,1,0:T(2,128)(2,1)} %copy-done.12, bf16[3,1408]{1,0:T(4,128)(2,1)} %refs_8_.1, bf16[3,1408]{1,0:T(4,128)(2,1)} %refs_9_.1), custom_call_target="tpu_custom_call" | custom-call | flops 9011200 | bytes 1048576 | tf_op jit(solution)/shard_map/pallas_call | solution.py:88
  10.8 8.5 %all-to-all-start = ((bf16[16,160,384]{2,1,0:T(8,128)(2,1)}), bf16[16,160,384]{2,1,0:T(8,128)(2,1)}, u32[]{:S(2)}, u32[]{:S(2)}) async-start(bf16[16,160,384]{2,1,0:T(8,128)(2,1)} %bitcast.19), calls=%async_computation | async-start | bytes 3932160 | tf_op jit(solution)/shard_map/all_to_all | solution.py:340
  19.3 3.4 %collective-permute-start.5 = (bf16[640,512]{1,0:T(8,128)(2,1)S(1)}, bf16[640,512]{1,0:T(8,128)(2,1)S(1)}, u32[]{:S(2)}, u32[]{:S(2)}) collective-permute-start(bf16[640,512]{1,0:T(8,128)(2,1)S(1)} %copy-done), channel_id=1, source_target_pairs={{0,64},{1,449},{8,72},{9,457},{16,80},{17,465},{24,88},{25,473},{3... | collective-permute-start | bytes 1966088 | tf_op jit(solution)/shard_map/ppermute | solution.py:331
  22.7 2.5 %collective-permute-start.6 = (bf16[640,512]{1,0:T(8,128)(2,1)S(1)}, bf16[640,512]{1,0:T(8,128)(2,1)S(1)}, u32[]{:S(2)}, u32[]{:S(2)}) collective-permute-start(bf16[640,512]{1,0:T(8,128)(2,1)S(1)} %copy-done), channel_id=1, source_target_pairs={{0,8},{1,57},{8,0},{9,17},{16,24},{17,9},{24,16},{25,33},{32,40},{... | collective-permute-start | bytes 1966088 | tf_op jit(solution)/shard_map/ppermute | solution.py:331
  25.2 3.4 %collective-permute-start.7 = (bf16[640,512]{1,0:T(8,128)(2,1)S(1)}, bf16[640,512]{1,0:T(8,128)(2,1)S(1)}, u32[]{:S(2)}, u32[]{:S(2)}) collective-permute-start(bf16[640,512]{1,0:T(8,128)(2,1)S(1)} %copy-done), channel_id=1, source_target_pairs={{0,72},{1,505},{8,64},{9,465},{16,88},{17,457},{24,80},{25,481},{3... | collective-permute-start | bytes 1966088 | tf_op jit(solution)/shard_map/ppermute | solution.py:331
  28.6 1.1 shard_map.112.order_ref
  29.8 0.5 copy-done.4
  30.3 21.5 %collective-permute-done.5.refs_1_ = bf16[640,512]{1,0:T(8,128)(2,1)S(1)} collective-permute-done((bf16[640,512]{1,0:T(8,128)(2,1)S(1)}, bf16[640,512]{1,0:T(8,128)(2,1)S(1)}, u32[]{:S(2)}, u32[]{:S(2)}) %collective-permute-start.5) | collective-permute-done | bytes 655392 | tf_op jit(solution)/shard_map/ppermute | solution.py:331
  52.0 0.7 copy-done.7
  52.6 0.3 copy-done.8
  53.0 5.5 %shard_map.113 = bf16[64,8,384]{2,1,0:T(8,128)(2,1)} custom-call(s32[4]{0:T(128)} %copy-done.4, bf16[640,512]{1,0:T(8,128)(2,1)} %refs_0_.1, bf16[640,512]{1,0:T(8,128)(2,1)} %copy-done.6, bf16[640,512]{1,0:T(8,128)(2,1)} %copy-done.7, bf16[640,512]{1,0:T(8,128)(2,1)} %copy-done.8, bf16[4,640,384]{2,1,0:T(8,128)(2,1)} %bitcast.13.refs_4_), custom_call_target="tpu_custom_call" | custom-call | flops 1006632960 | bytes 1048576 | tf_op jit(solution)/shard_map/pallas_call | solution.py:179
  58.5 17.8 %all-to-all-start.1 = ((bf16[64,8,384]{2,1,0:T(8,128)(2,1)}), bf16[64,8,384]{2,1,0:T(8,128)(2,1)S(1)}, u32[]{:S(2)}, u32[]{:S(2)}) async-start(bf16[64,8,384]{2,1,0:T(8,128)(2,1)} %shard_map.113), calls=%async_computation.1 | async-start | bytes 786432 | tf_op jit(solution)/shard_map/all_to_all | solution.py:32
  76.5 1.4 copy-done.5
  77.8 2.5 %shard_map.110 = (bf16[168,1408]{1,0:T(8,128)(2,1)S(1)}, bf16[168,1408]{1,0:T(8,128)(2,1)S(1)}, bf16[168,1408]{1,0:T(8,128)(2,1)S(1)}, bf16[168,1408]{1,0:T(8,128)(2,1)S(1)}) custom-call(s32[4]{0:T(128)S(1)} %pad_add_fusion.at_ref, bf16[640,512]{1,0:T(8,128)(2,1)S(1)} %copy-done.1, bf16[1408,512]{1,0:T(8,128)(2,1)S(1)} %copy-done.5), custom_call_target="tpu_custom_call" | custom-call | flops 922746880 | bytes 1048576 | tf_op jit(solution)/shard_map/pallas_call | solution.py:120
  80.3 0.8 copy-done.2
  81.1 3.5 %collective-permute-start.1 = (bf16[168,1408]{1,0:T(8,128)(2,1)S(1)}, bf16[168,1408]{1,0:T(8,128)(2,1)S(1)}, u32[]{:S(2)}, u32[]{:S(2)}) collective-permute-start(bf16[168,1408]{1,0:T(8,128)(2,1)S(1)} %get-tuple-element.20), channel_id=1, source_target_pairs={{0,2},{2,4},{4,6},{6,0},{1,3},{3,5},{5,7},{7,1},{8,10},{10,12},{12... | collective-permute-start | bytes 1419272 | tf_op jit(solution)/shard_map/ppermute | solution.py:356
  84.6 3.6 %collective-permute-start.2 = (bf16[168,1408]{1,0:T(8,128)(2,1)S(1)}, bf16[168,1408]{1,0:T(8,128)(2,1)S(1)}, u32[]{:S(2)}, u32[]{:S(2)}) collective-permute-start(bf16[168,1408]{1,0:T(8,128)(2,1)S(1)} %get-tuple-element.21), channel_id=1, source_target_pairs={{0,6},{2,0},{4,2},{6,4},{1,7},{3,1},{5,3},{7,5},{8,14},{10,8},{12,... | collective-permute-start | bytes 1419272 | tf_op jit(solution)/shard_map/ppermute | solution.py:356
  88.2 2.4 %collective-permute-start.3 = (bf16[168,1408]{1,0:T(8,128)(2,1)S(1)}, bf16[168,1408]{1,0:T(8,128)(2,1)S(1)}, u32[]{:S(2)}, u32[]{:S(2)}) collective-permute-start(bf16[168,1408]{1,0:T(8,128)(2,1)S(1)} %get-tuple-element.22), channel_id=1, source_target_pairs={{0,4},{2,6},{4,0},{6,2},{1,5},{3,7},{5,1},{7,3},{8,12},{10,14},{12... | collective-permute-start | bytes 1419272 | tf_op jit(solution)/shard_map/ppermute | solution.py:356
  90.6 1.3 collective-permute-start.4
  91.9 12.3 %collective-permute-done.4.refs_7_ = bf16[2,2,1408]{2,1,0:T(2,128)(2,1)S(1)} collective-permute-done((bf16[2,2,1408]{2,1,0:T(2,128)(2,1)S(1)}, bf16[2,2,1408]{2,1,0:T(2,128)(2,1)S(1)}, u32[]{:S(2)}, u32[]{:S(2)}) %collective-permute-start.4) | collective-permute-done | bytes 11296 | tf_op jit(solution)/shard_map/ppermute | solution.py:28
  104.2 0.6 copy-done.13
  105.3 5.1 %shard_map.111 = (bf16[160,1408]{1,0:T(8,128)(2,1)}, bf16[160,1408]{1,0:T(8,128)(2,1)}, f32[8,1408]{1,0:T(8,128)}) custom-call(bf16[168,1408]{1,0:T(8,128)(2,1)} %copy-done.9, bf16[168,1408]{1,0:T(8,128)(2,1)} %copy-done.10, bf16[168,1408]{1,0:T(8,128)(2,1)} %copy-done.11, bf16[168,1408]{1,0:T(8,128)(2,1)} %copy-done.2, bf16[160,1408]{1,0:T(8,128)(2,1)} %refs_4_.1, ...), custom_call_target="tpu_custom_call" | custom-call | flops 22528000 | bytes 1048576 | tf_op jit(solution)/shard_map/pallas_call | solution.py:273
  110.4 0.8 copy-done.3
  111.2 0.7 shard_map.114
  111.9 11.9 %all_to_all.25.seen_ref = bf16[16,8,384]{2,1,0:T(8,128)(2,1)S(1)} all-to-all(bf16[16,8,384]{2,1,0:T(8,128)(2,1)S(1)} %get-tuple-element.27), channel_id=1, replica_groups=mesh['zh'=4,'zl'=2,'yh'=4,'yl'=2,'fs'=4,'tp'=2] {'zl','yl','fs'}, dimensions={0} | all-to-all | bytes 196608 | tf_op jit(solution)/shard_map/all_to_all | solution.py:32
  123.8 22.2 %all_to_all.26.seen_ref = bf16[16,8,384]{2,1,0:T(8,128)(2,1)S(1)} all-to-all(bf16[16,8,384]{2,1,0:T(8,128)(2,1)S(1)} %shard_map.115), channel_id=1, replica_groups=mesh['zh'=4,'zl'=2,'yh'=4,'yl'=2,'fs'=4,'tp'=2] {'zh','yh'}, dimensions={0} | all-to-all | bytes 196608 | tf_op jit(solution)/shard_map/all_to_all | solution.py:32
  146.0 7.6 %all_to_all.27.seen_ref = f32[4,8,384]{2,1,0:T(8,128)S(1)} all-to-all(f32[4,8,384]{2,1,0:T(8,128)S(1)} %shard_map.116), channel_id=1, replica_groups=mesh['zh'=4,'zl'=2,'yh'=4,'yl'=2,'fs'=4,'tp'=2] {'zl','yl'}, dimensions={0} | all-to-all | bytes 98304 | tf_op jit(solution)/shard_map/all_to_all | solution.py:32
  153.7 0.6 shard_map.117
  (33 shorter events, 1.1 us)
Async XLA Ops:
  1.5 4.8 %collective-permute-start = (bf16[2,2,1408]{2,1,0:T(2,128)(2,1)S(1)}, bf16[2,2,1408]{2,1,0:T(2,128)(2,1)S(1)}, u32[]{:S(2)}, u32[]{:S(2)}) collective-permute-start(bf16[2,2,1408]{2,1,0:T(2,128)(2,1)S(1)} %pad_maximum_fusion), channel_id=1, source_target_pairs={{0,2},{2,4},{4,6},{1,3},{3,5},{5,7},{8,10},{10,12},{12,14},{9,11},... | collective-permute-start | bytes 33800 | tf_op jit(solution)/shard_map/ppermute | solution.py:28
  6.3 0.6 copy-start.12
  10.8 8.5 %copy-start = (bf16[640,512]{1,0:T(8,128)(2,1)S(1)}, bf16[640,512]{1,0:T(8,128)(2,1)}, u32[]{:S(2)}) copy-start(bf16[640,512]{1,0:T(8,128)(2,1)} %refs_0_.1) | copy-start | bytes 1966084
  10.8 41.2 %all-to-all-start = ((bf16[16,160,384]{2,1,0:T(8,128)(2,1)}), bf16[16,160,384]{2,1,0:T(8,128)(2,1)}, u32[]{:S(2)}, u32[]{:S(2)}) async-start(bf16[16,160,384]{2,1,0:T(8,128)(2,1)} %bitcast.19), calls=%async_computation | async-start | bytes 3932160 | tf_op jit(solution)/shard_map/all_to_all | solution.py:340
  19.3 32.5 %collective-permute-start.5 = (bf16[640,512]{1,0:T(8,128)(2,1)S(1)}, bf16[640,512]{1,0:T(8,128)(2,1)S(1)}, u32[]{:S(2)}, u32[]{:S(2)}) collective-permute-start(bf16[640,512]{1,0:T(8,128)(2,1)S(1)} %copy-done), channel_id=1, source_target_pairs={{0,64},{1,449},{8,72},{9,457},{16,80},{17,465},{24,88},{25,473},{3... | collective-permute-start | bytes 1966088 | tf_op jit(solution)/shard_map/ppermute | solution.py:331
  22.7 29.1 %collective-permute-start.6 = (bf16[640,512]{1,0:T(8,128)(2,1)S(1)}, bf16[640,512]{1,0:T(8,128)(2,1)S(1)}, u32[]{:S(2)}, u32[]{:S(2)}) collective-permute-start(bf16[640,512]{1,0:T(8,128)(2,1)S(1)} %copy-done), channel_id=1, source_target_pairs={{0,8},{1,57},{8,0},{9,17},{16,24},{17,9},{24,16},{25,33},{32,40},{... | collective-permute-start | bytes 1966088 | tf_op jit(solution)/shard_map/ppermute | solution.py:331
  25.2 26.8 %collective-permute-start.7 = (bf16[640,512]{1,0:T(8,128)(2,1)S(1)}, bf16[640,512]{1,0:T(8,128)(2,1)S(1)}, u32[]{:S(2)}, u32[]{:S(2)}) collective-permute-start(bf16[640,512]{1,0:T(8,128)(2,1)S(1)} %copy-done), channel_id=1, source_target_pairs={{0,72},{1,505},{8,64},{9,465},{16,88},{17,457},{24,80},{25,481},{3... | collective-permute-start | bytes 1966088 | tf_op jit(solution)/shard_map/ppermute | solution.py:331
  29.8 0.5 copy-start.4
  51.8 1.3 copy-start.6
  51.8 0.9 copy-start.7
  52.0 1.0 copy-start.8
  53.0 23.4 %copy-start.1 = (bf16[640,512]{1,0:T(8,128)(2,1)S(1)}, bf16[640,512]{1,0:T(8,128)(2,1)}, u32[]{:S(2)}) copy-start(bf16[640,512]{1,0:T(8,128)(2,1)} %refs_0_.1) | copy-start | bytes 1966084
  58.5 51.9 %all-to-all-start.1 = ((bf16[64,8,384]{2,1,0:T(8,128)(2,1)}), bf16[64,8,384]{2,1,0:T(8,128)(2,1)S(1)}, u32[]{:S(2)}, u32[]{:S(2)}) async-start(bf16[64,8,384]{2,1,0:T(8,128)(2,1)} %shard_map.113), calls=%async_computation.1 | async-start | bytes 786432 | tf_op jit(solution)/shard_map/all_to_all | solution.py:32
  76.5 1.4 copy-start.5
  80.3 0.8 copy-start.2
  81.1 23.1 %collective-permute-start.1 = (bf16[168,1408]{1,0:T(8,128)(2,1)S(1)}, bf16[168,1408]{1,0:T(8,128)(2,1)S(1)}, u32[]{:S(2)}, u32[]{:S(2)}) collective-permute-start(bf16[168,1408]{1,0:T(8,128)(2,1)S(1)} %get-tuple-element.20), channel_id=1, source_target_pairs={{0,2},{2,4},{4,6},{6,0},{1,3},{3,5},{5,7},{7,1},{8,10},{10,12},{12... | collective-permute-start | bytes 1419272 | tf_op jit(solution)/shard_map/ppermute | solution.py:356
  84.6 19.6 %collective-permute-start.2 = (bf16[168,1408]{1,0:T(8,128)(2,1)S(1)}, bf16[168,1408]{1,0:T(8,128)(2,1)S(1)}, u32[]{:S(2)}, u32[]{:S(2)}) collective-permute-start(bf16[168,1408]{1,0:T(8,128)(2,1)S(1)} %get-tuple-element.21), channel_id=1, source_target_pairs={{0,6},{2,0},{4,2},{6,4},{1,7},{3,1},{5,3},{7,5},{8,14},{10,8},{12,... | collective-permute-start | bytes 1419272 | tf_op jit(solution)/shard_map/ppermute | solution.py:356
  88.2 16.1 %collective-permute-start.3 = (bf16[168,1408]{1,0:T(8,128)(2,1)S(1)}, bf16[168,1408]{1,0:T(8,128)(2,1)S(1)}, u32[]{:S(2)}, u32[]{:S(2)}) collective-permute-start(bf16[168,1408]{1,0:T(8,128)(2,1)S(1)} %get-tuple-element.22), channel_id=1, source_target_pairs={{0,4},{2,6},{4,0},{6,2},{1,5},{3,7},{5,1},{7,3},{8,12},{10,14},{12... | collective-permute-start | bytes 1419272 | tf_op jit(solution)/shard_map/ppermute | solution.py:356
  90.6 13.6 %collective-permute-start.4 = (bf16[2,2,1408]{2,1,0:T(2,128)(2,1)S(1)}, bf16[2,2,1408]{2,1,0:T(2,128)(2,1)S(1)}, u32[]{:S(2)}, u32[]{:S(2)}) collective-permute-start(bf16[2,2,1408]{2,1,0:T(2,128)(2,1)S(1)} %pad_maximum_fusion.1), channel_id=1, source_target_pairs={{2,0},{4,2},{6,4},{3,1},{5,3},{7,5},{10,8},{12,10},{14,12},{11,9},... | collective-permute-start | bytes 33800 | tf_op jit(solution)/shard_map/ppermute | solution.py:28
  104.2 0.6 copy-start.13
  104.2 0.8 copy-start.9
  104.2 0.9 copy-start.10
  104.2 1.1 copy-start.11
  110.4 0.8 copy-start.3

commit v5 on v4

--- a/solution.py
+++ b/solution.py
@@ -193,10 +193,13 @@
     )(order, *blocks, hidden)
 
 
+def keep_body(taps_ref, out_ref):
+    out_ref[...] = taps_ref[...]
+
+
 def share_body(scale, parts_ref, taps_ref, grad_ref, small_ref):
     block = parts_ref.shape[2]
-    rows, width = taps_ref.shape
-    copies = small_ref.shape[0] // GROUP
+    copies, rows, width = small_ref.shape
     for zl in range(2):
         for yl in range(2):
             total = None
@@ -211,13 +214,8 @@
     norm = jnp.sum(value * value, axis=0, keepdims=True)
     row = lax.broadcasted_iota(jnp.int32, (rows, width), 0)
     small = jnp.where(row == rows - 1, norm, taps_ref[...]).astype(BF16)
-    for member in range(GROUP):
-        start = member * block
-        size = min(block, width - start)
-        for k in range(member * copies, (member + 1) * copies):
-            small_ref[k, :, :size] = small[:, start : start + size]
-            if size < block:
-                small_ref[k, :, size:] = jnp.zeros((rows, block - size), BF16)
+    for k in range(copies):
+        small_ref[k] = small
 
 
 def chain_body(rows, *refs):
@@ -292,20 +290,16 @@
 
 
 def middle_body(seen_ref, small_ref):
-    total = total_of(seen_ref).astype(small_ref.dtype)
+    total = total_of(seen_ref).astype(BF16)
     for k in range(small_ref.shape[0]):
         small_ref[k] = total
 
 
 def last_body(scale, seen_ref, gate_ref, up_ref, norm_ref):
-    block = seen_ref.shape[2]
-    for member in range(GROUP):
-        start = member * block
-        size = min(block, gate_ref.shape[1] - start)
-        lanes = slice(start, start + size)
-        gate_ref[:, lanes] = seen_ref[member, :3, :size] * scale
-        up_ref[:, lanes] = seen_ref[member, 3:6, :size] * scale
-        norm_ref[lanes] = seen_ref[member, 7, :size] / D
+    total = total_of(seen_ref)
+    gate_ref[...] = total[:3] * scale
+    up_ref[...] = total[3:6] * scale
+    norm_ref[...] = total[7] / D
 
 
 def local(gate_pre, up_pre, gate_taps, up_taps, down_weight, cotangent):
@@ -362,17 +356,18 @@
         terms, gate_pre, up_pre, before, after, gate_taps, up_taps, block
     )
 
-    sent = jax.ShapeDtypeStruct((n_near, 8, block), BF16)
+    wide = jax.ShapeDtypeStruct((8, width), F32)
+    taps = call(keep_body, wide)(taps)
+    sent = functools.partial(jax.ShapeDtypeStruct, dtype=BF16)
     grad_share, small = call(
-        functools.partial(share_body, grad_scale), (jax.ShapeDtypeStruct((8, width), F32), sent)
+        functools.partial(share_body, grad_scale), (wide, sent((n_near, 8, width)))
     )(parts, taps)
-    small = call(middle_body, jax.ShapeDtypeStruct((n_far, 8, block), BF16))(swap(small, NEAR))
-    small = call(middle_body, jax.ShapeDtypeStruct((GROUP, 8, block), F32))(swap(small, FAR))
+    small = call(middle_body, sent((n_far, 8, width)))(swap(small, NEAR))
     three = jax.ShapeDtypeStruct((3, width), F32)
     gate_out, up_out, norms = call(
         functools.partial(last_body, grad_scale),
         (three, three, jax.ShapeDtypeStruct((width,), F32)),
-    )(swap(small, ("zl", "yl")))
+    )(swap(small, FAR))
     return grad_gate, grad_up, gate_out, up_out, grad_share[None], norms
 
 

time: 155 us -> 151 us (0.974)
  the two profiles are of different devices: /device:TPU:8 before, /device:TPU:16 now
where the time goes in v5:
time: 151 us; the launch traced here: 150 us
  starting transfers between devices  47.2 us (31%)
  waiting for transfers between devices  37.9 us (25%)
  blocking collectives  37.9 us (25%)
  Pallas kernels  19.6 us (13%)
  local copies, waits for them, and re-layouts  6.76 us (4%)
    all_to_all x2, blocking collectives, swap(): return lax.all_to_all(array, axes, 0, 0, tiled=True)  37.9 us
    ppermute x3, waiting for transfers between devices, collected(): return lax.ppermute(cotangent, ZY + ('tp',), pairs)  24.1 us
    all_to_all x1, starting transfers between devices, swap(): return lax.all_to_all(array, axes, 0, 0, tiled=True)  15.7 us
    ppermute x2, waiting for transfers between devices, passed_along(): return lax.ppermute(array, axis, pairs)  13.7 us
    ppermute x3, starting transfers between devices, local(): terms[k] = lax.ppermute(terms[k], 'fs', pairs)  9.41 us
    ppermute x3, starting transfers between devices, collected(): return lax.ppermute(cotangent, ZY + ('tp',), pairs)  9.21 us
    all_to_all x1, starting transfers between devices, local(): lax.all_to_all(hidden.reshape(n_near, rows, block), TOK + ('tp',), 0, 0,...  8.2 us
    unnamed x28, local copies, waits for them, and re-layouts  5.95 us
  transfers between devices with their start and end apart: 10, of which 5 were waited for; matrix products, arithmetic and copies ran while one was open for 0% of the time, Pallas kernels for 6%

profile of v5, /device:TPU:16, one launch (start us, length us, event | category | flops | bytes accessed | tf_op | source)
XLA Modules:
  0.0 150.4 jit_solution(9871962297467111971)
XLA Ops:
  0.6 0.8 slice_bitcast_fusion
  1.5 3.4 %collective-permute-start = (bf16[2,2,1408]{2,1,0:T(2,128)(2,1)S(1)}, bf16[2,2,1408]{2,1,0:T(2,128)(2,1)S(1)}, u32[]{:S(2)}, u32[]{:S(2)}) collective-permute-start(bf16[2,2,1408]{2,1,0:T(2,128)(2,1)S(1)} %pad_maximum_fusion), channel_id=1, source_target_pairs={{0,2},{2,4},{4,6},{1,3},{3,5},{5,7},{8,10},{10,12},{12,14},{9,11},... | collective-permute-start | bytes 33800 | tf_op jit(solution)/shard_map/ppermute | solution.py:28
  4.9 1.4 collective-permute-done.before_ref.refs_6_
  6.3 0.6 copy-done.12
  6.9 3.9 %shard_map.109 = bf16[4,4,160,384]{3,2,1,0:T(8,128)(2,1)} custom-call(bf16[160,1408]{1,0:T(8,128)(2,1)} %refs_4_.1, bf16[160,1408]{1,0:T(8,128)(2,1)} %refs_5_.1, bf16[2,2,1408]{2,1,0:T(2,128)(2,1)} %copy-done.12, bf16[3,1408]{1,0:T(4,128)(2,1)} %refs_8_.1, bf16[3,1408]{1,0:T(4,128)(2,1)} %refs_9_.1), custom_call_target="tpu_custom_call" | custom-call | flops 9011200 | bytes 1048576 | tf_op jit(solution)/shard_map/pallas_call | solution.py:88
  10.8 8.2 %all-to-all-start = ((bf16[16,160,384]{2,1,0:T(8,128)(2,1)}), bf16[16,160,384]{2,1,0:T(8,128)(2,1)}, u32[]{:S(2)}, u32[]{:S(2)}) async-start(bf16[16,160,384]{2,1,0:T(8,128)(2,1)} %bitcast.19), calls=%async_computation | async-start | bytes 3932160 | tf_op jit(solution)/shard_map/all_to_all | solution.py:334
  19.0 3.8 %collective-permute-start.5 = (bf16[640,512]{1,0:T(8,128)(2,1)S(1)}, bf16[640,512]{1,0:T(8,128)(2,1)S(1)}, u32[]{:S(2)}, u32[]{:S(2)}) collective-permute-start(bf16[640,512]{1,0:T(8,128)(2,1)S(1)} %copy-done), channel_id=1, source_target_pairs={{0,64},{1,449},{8,72},{9,457},{16,80},{17,465},{24,88},{25,473},{3... | collective-permute-start | bytes 1966088 | tf_op jit(solution)/shard_map/ppermute | solution.py:325
  22.8 3.4 %collective-permute-start.6 = (bf16[640,512]{1,0:T(8,128)(2,1)S(1)}, bf16[640,512]{1,0:T(8,128)(2,1)S(1)}, u32[]{:S(2)}, u32[]{:S(2)}) collective-permute-start(bf16[640,512]{1,0:T(8,128)(2,1)S(1)} %copy-done), channel_id=1, source_target_pairs={{0,8},{1,57},{8,0},{9,17},{16,24},{17,9},{24,16},{25,33},{32,40},{... | collective-permute-start | bytes 1966088 | tf_op jit(solution)/shard_map/ppermute | solution.py:325
  26.2 2.1 %collective-permute-start.7 = (bf16[640,512]{1,0:T(8,128)(2,1)S(1)}, bf16[640,512]{1,0:T(8,128)(2,1)S(1)}, u32[]{:S(2)}, u32[]{:S(2)}) collective-permute-start(bf16[640,512]{1,0:T(8,128)(2,1)S(1)} %copy-done), channel_id=1, source_target_pairs={{0,72},{1,505},{8,64},{9,465},{16,88},{17,457},{24,80},{25,481},{3... | collective-permute-start | bytes 1966088 | tf_op jit(solution)/shard_map/ppermute | solution.py:325
  28.3 1.1 shard_map.112.order_ref
  29.5 0.5 copy-done.4
  30.0 14.4 %collective-permute-done.5.refs_1_ = bf16[640,512]{1,0:T(8,128)(2,1)S(1)} collective-permute-done((bf16[640,512]{1,0:T(8,128)(2,1)S(1)}, bf16[640,512]{1,0:T(8,128)(2,1)S(1)}, u32[]{:S(2)}, u32[]{:S(2)}) %collective-permute-start.5) | collective-permute-done | bytes 655392 | tf_op jit(solution)/shard_map/ppermute | solution.py:325
  44.4 2.1 %collective-permute-done.6.refs_2_ = bf16[640,512]{1,0:T(8,128)(2,1)S(1)} collective-permute-done((bf16[640,512]{1,0:T(8,128)(2,1)S(1)}, bf16[640,512]{1,0:T(8,128)(2,1)S(1)}, u32[]{:S(2)}, u32[]{:S(2)}) %collective-permute-start.6) | collective-permute-done | bytes 655392 | tf_op jit(solution)/shard_map/ppermute | solution.py:325
  46.4 7.7 %collective-permute-done.7.refs_3_ = bf16[640,512]{1,0:T(8,128)(2,1)S(1)} collective-permute-done((bf16[640,512]{1,0:T(8,128)(2,1)S(1)}, bf16[640,512]{1,0:T(8,128)(2,1)S(1)}, u32[]{:S(2)}, u32[]{:S(2)}) %collective-permute-start.7) | collective-permute-done | bytes 655392 | tf_op jit(solution)/shard_map/ppermute | solution.py:325
  54.1 0.8 copy-done.8
  55.0 5.5 %shard_map.113 = bf16[64,8,384]{2,1,0:T(8,128)(2,1)} custom-call(s32[4]{0:T(128)} %copy-done.4, bf16[640,512]{1,0:T(8,128)(2,1)} %refs_0_.1, bf16[640,512]{1,0:T(8,128)(2,1)} %copy-done.6, bf16[640,512]{1,0:T(8,128)(2,1)} %copy-done.7, bf16[640,512]{1,0:T(8,128)(2,1)} %copy-done.8, bf16[4,640,384]{2,1,0:T(8,128)(2,1)} %bitcast.13.refs_4_), custom_call_target="tpu_custom_call" | custom-call | flops 1006632960 | bytes 1048576 | tf_op jit(solution)/shard_map/pallas_call | solution.py:179
  60.5 15.7 %all-to-all-start.1 = ((bf16[64,8,384]{2,1,0:T(8,128)(2,1)}), bf16[64,8,384]{2,1,0:T(8,128)(2,1)S(1)}, u32[]{:S(2)}, u32[]{:S(2)}) async-start(bf16[64,8,384]{2,1,0:T(8,128)(2,1)} %shard_map.113), calls=%async_computation.1 | async-start | bytes 786432 | tf_op jit(solution)/shard_map/all_to_all | solution.py:32
  76.3 1.4 copy-done.5
  77.7 2.5 %shard_map.110 = (bf16[168,1408]{1,0:T(8,128)(2,1)S(1)}, bf16[168,1408]{1,0:T(8,128)(2,1)S(1)}, bf16[168,1408]{1,0:T(8,128)(2,1)S(1)}, bf16[168,1408]{1,0:T(8,128)(2,1)S(1)}) custom-call(s32[4]{0:T(128)S(1)} %pad_add_fusion.at_ref, bf16[640,512]{1,0:T(8,128)(2,1)S(1)} %copy-done.1, bf16[1408,512]{1,0:T(8,128)(2,1)S(1)} %copy-done.5), custom_call_target="tpu_custom_call" | custom-call | flops 922746880 | bytes 1048576 | tf_op jit(solution)/shard_map/pallas_call | solution.py:120
  80.2 0.8 copy-done.2
  81.0 3.5 %collective-permute-start.1 = (bf16[168,1408]{1,0:T(8,128)(2,1)S(1)}, bf16[168,1408]{1,0:T(8,128)(2,1)S(1)}, u32[]{:S(2)}, u32[]{:S(2)}) collective-permute-start(bf16[168,1408]{1,0:T(8,128)(2,1)S(1)} %get-tuple-element.20), channel_id=1, source_target_pairs={{0,2},{2,4},{4,6},{6,0},{1,3},{3,5},{5,7},{7,1},{8,10},{10,12},{12... | collective-permute-start | bytes 1419272 | tf_op jit(solution)/shard_map/ppermute | solution.py:350
  84.5 3.6 %collective-permute-start.2 = (bf16[168,1408]{1,0:T(8,128)(2,1)S(1)}, bf16[168,1408]{1,0:T(8,128)(2,1)S(1)}, u32[]{:S(2)}, u32[]{:S(2)}) collective-permute-start(bf16[168,1408]{1,0:T(8,128)(2,1)S(1)} %get-tuple-element.21), channel_id=1, source_target_pairs={{0,6},{2,0},{4,2},{6,4},{1,7},{3,1},{5,3},{7,5},{8,14},{10,8},{12,... | collective-permute-start | bytes 1419272 | tf_op jit(solution)/shard_map/ppermute | solution.py:350
  88.0 2.4 %collective-permute-start.3 = (bf16[168,1408]{1,0:T(8,128)(2,1)S(1)}, bf16[168,1408]{1,0:T(8,128)(2,1)S(1)}, u32[]{:S(2)}, u32[]{:S(2)}) collective-permute-start(bf16[168,1408]{1,0:T(8,128)(2,1)S(1)} %get-tuple-element.22), channel_id=1, source_target_pairs={{0,4},{2,6},{4,0},{6,2},{1,5},{3,7},{5,1},{7,3},{8,12},{10,14},{12... | collective-permute-start | bytes 1419272 | tf_op jit(solution)/shard_map/ppermute | solution.py:350
  90.4 1.3 collective-permute-start.4
  91.7 12.3 %collective-permute-done.4.refs_7_ = bf16[2,2,1408]{2,1,0:T(2,128)(2,1)S(1)} collective-permute-done((bf16[2,2,1408]{2,1,0:T(2,128)(2,1)S(1)}, bf16[2,2,1408]{2,1,0:T(2,128)(2,1)S(1)}, u32[]{:S(2)}, u32[]{:S(2)}) %collective-permute-start.4) | collective-permute-done | bytes 11296 | tf_op jit(solution)/shard_map/ppermute | solution.py:28
  104.1 0.6 copy-done.13
  105.2 5.1 %shard_map.111 = (bf16[160,1408]{1,0:T(8,128)(2,1)}, bf16[160,1408]{1,0:T(8,128)(2,1)}, f32[8,1408]{1,0:T(8,128)}) custom-call(bf16[168,1408]{1,0:T(8,128)(2,1)} %copy-done.9, bf16[168,1408]{1,0:T(8,128)(2,1)} %copy-done.10, bf16[168,1408]{1,0:T(8,128)(2,1)} %copy-done.11, bf16[168,1408]{1,0:T(8,128)(2,1)} %copy-done.2, bf16[160,1408]{1,0:T(8,128)(2,1)} %refs_4_.1, ...), custom_call_target="tpu_custom_call" | custom-call | flops 22528000 | bytes 1048576 | tf_op jit(solution)/shard_map/pallas_call | solution.py:271
  110.3 0.8 copy-done.3
  111.1 0.7 shard_map.115
  111.8 14.5 %all_to_all.20.seen_ref = bf16[16,8,1408]{2,1,0:T(8,128)(2,1)S(1)} all-to-all(bf16[16,8,1408]{2,1,0:T(8,128)(2,1)S(1)} %get-tuple-element.27), channel_id=1, replica_groups=mesh['zh'=4,'zl'=2,'yh'=4,'yl'=2,'fs'=4,'tp'=2] {'zl','yl','fs'}, dimensions={0} | all-to-all | bytes 720896 | tf_op jit(solution)/shard_map/all_to_all | solution.py:32
  126.3 23.4 %all_to_all.21.seen_ref = bf16[16,8,1408]{2,1,0:T(8,128)(2,1)S(1)} all-to-all(bf16[16,8,1408]{2,1,0:T(8,128)(2,1)S(1)} %shard_map.116), channel_id=1, replica_groups=mesh['zh'=4,'zl'=2,'yh'=4,'yl'=2,'fs'=4,'tp'=2] {'zh','yh'}, dimensions={0} | all-to-all | bytes 720896 | tf_op jit(solution)/shard_map/all_to_all | solution.py:32
  149.7 0.7 shard_map.117
  (32 shorter events, 0.8 us)
Async XLA Ops:
  1.5 4.8 %collective-permute-start = (bf16[2,2,1408]{2,1,0:T(2,128)(2,1)S(1)}, bf16[2,2,1408]{2,1,0:T(2,128)(2,1)S(1)}, u32[]{:S(2)}, u32[]{:S(2)}) collective-permute-start(bf16[2,2,1408]{2,1,0:T(2,128)(2,1)S(1)} %pad_maximum_fusion), channel_id=1, source_target_pairs={{0,2},{2,4},{4,6},{1,3},{3,5},{5,7},{8,10},{10,12},{12,14},{9,11},... | collective-permute-start | bytes 33800 | tf_op jit(solution)/shard_map/ppermute | solution.py:28
  6.3 0.6 copy-start.12
  10.8 8.2 %copy-start = (bf16[640,512]{1,0:T(8,128)(2,1)S(1)}, bf16[640,512]{1,0:T(8,128)(2,1)}, u32[]{:S(2)}) copy-start(bf16[640,512]{1,0:T(8,128)(2,1)} %refs_0_.1) | copy-start | bytes 1966084
  10.8 43.3 %all-to-all-start = ((bf16[16,160,384]{2,1,0:T(8,128)(2,1)}), bf16[16,160,384]{2,1,0:T(8,128)(2,1)}, u32[]{:S(2)}, u32[]{:S(2)}) async-start(bf16[16,160,384]{2,1,0:T(8,128)(2,1)} %bitcast.19), calls=%async_computation | async-start | bytes 3932160 | tf_op jit(solution)/shard_map/all_to_all | solution.py:334
  19.0 25.4 %collective-permute-start.5 = (bf16[640,512]{1,0:T(8,128)(2,1)S(1)}, bf16[640,512]{1,0:T(8,128)(2,1)S(1)}, u32[]{:S(2)}, u32[]{:S(2)}) collective-permute-start(bf16[640,512]{1,0:T(8,128)(2,1)S(1)} %copy-done), channel_id=1, source_target_pairs={{0,64},{1,449},{8,72},{9,457},{16,80},{17,465},{24,88},{25,473},{3... | collective-permute-start | bytes 1966088 | tf_op jit(solution)/shard_map/ppermute | solution.py:325
  22.8 23.6 %collective-permute-start.6 = (bf16[640,512]{1,0:T(8,128)(2,1)S(1)}, bf16[640,512]{1,0:T(8,128)(2,1)S(1)}, u32[]{:S(2)}, u32[]{:S(2)}) collective-permute-start(bf16[640,512]{1,0:T(8,128)(2,1)S(1)} %copy-done), channel_id=1, source_target_pairs={{0,8},{1,57},{8,0},{9,17},{16,24},{17,9},{24,16},{25,33},{32,40},{... | collective-permute-start | bytes 1966088 | tf_op jit(solution)/shard_map/ppermute | solution.py:325
  26.2 27.9 %collective-permute-start.7 = (bf16[640,512]{1,0:T(8,128)(2,1)S(1)}, bf16[640,512]{1,0:T(8,128)(2,1)S(1)}, u32[]{:S(2)}, u32[]{:S(2)}) collective-permute-start(bf16[640,512]{1,0:T(8,128)(2,1)S(1)} %copy-done), channel_id=1, source_target_pairs={{0,72},{1,505},{8,64},{9,465},{16,88},{17,457},{24,80},{25,481},{3... | collective-permute-start | bytes 1966088 | tf_op jit(solution)/shard_map/ppermute | solution.py:325
  29.5 0.5 copy-start.4
  44.4 10.6 %copy-start.6 = (bf16[640,512]{1,0:T(8,128)(2,1)}, bf16[640,512]{1,0:T(8,128)(2,1)S(1)}, u32[]{:S(2)}) copy-start(bf16[640,512]{1,0:T(8,128)(2,1)S(1)} %collective-permute-done.5.refs_1_) | copy-start | bytes 1966084
  46.4 7.7 %copy-start.7 = (bf16[640,512]{1,0:T(8,128)(2,1)}, bf16[640,512]{1,0:T(8,128)(2,1)S(1)}, u32[]{:S(2)}) copy-start(bf16[640,512]{1,0:T(8,128)(2,1)S(1)} %collective-permute-done.6.refs_2_) | copy-start | bytes 1966084
  54.1 0.8 copy-start.8
  55.0 21.4 %copy-start.1 = (bf16[640,512]{1,0:T(8,128)(2,1)S(1)}, bf16[640,512]{1,0:T(8,128)(2,1)}, u32[]{:S(2)}) copy-start(bf16[640,512]{1,0:T(8,128)(2,1)} %refs_0_.1) | copy-start | bytes 1966084
  60.5 50.6 %all-to-all-start.1 = ((bf16[64,8,384]{2,1,0:T(8,128)(2,1)}), bf16[64,8,384]{2,1,0:T(8,128)(2,1)S(1)}, u32[]{:S(2)}, u32[]{:S(2)}) async-start(bf16[64,8,384]{2,1,0:T(8,128)(2,1)} %shard_map.113), calls=%async_computation.1 | async-start | bytes 786432 | tf_op jit(solution)/shard_map/all_to_all | solution.py:32
  76.3 1.4 copy-start.5
  80.2 0.8 copy-start.2
  81.0 23.1 %collective-permute-start.1 = (bf16[168,1408]{1,0:T(8,128)(2,1)S(1)}, bf16[168,1408]{1,0:T(8,128)(2,1)S(1)}, u32[]{:S(2)}, u32[]{:S(2)}) collective-permute-start(bf16[168,1408]{1,0:T(8,128)(2,1)S(1)} %get-tuple-element.20), channel_id=1, source_target_pairs={{0,2},{2,4},{4,6},{6,0},{1,3},{3,5},{5,7},{7,1},{8,10},{10,12},{12... | collective-permute-start | bytes 1419272 | tf_op jit(solution)/shard_map/ppermute | solution.py:350
  84.5 19.6 %collective-permute-start.2 = (bf16[168,1408]{1,0:T(8,128)(2,1)S(1)}, bf16[168,1408]{1,0:T(8,128)(2,1)S(1)}, u32[]{:S(2)}, u32[]{:S(2)}) collective-permute-start(bf16[168,1408]{1,0:T(8,128)(2,1)S(1)} %get-tuple-element.21), channel_id=1, source_target_pairs={{0,6},{2,0},{4,2},{6,4},{1,7},{3,1},{5,3},{7,5},{8,14},{10,8},{12,... | collective-permute-start | bytes 1419272 | tf_op jit(solution)/shard_map/ppermute | solution.py:350
  88.0 16.1 %collective-permute-start.3 = (bf16[168,1408]{1,0:T(8,128)(2,1)S(1)}, bf16[168,1408]{1,0:T(8,128)(2,1)S(1)}, u32[]{:S(2)}, u32[]{:S(2)}) collective-permute-start(bf16[168,1408]{1,0:T(8,128)(2,1)S(1)} %get-tuple-element.22), channel_id=1, source_target_pairs={{0,4},{2,6},{4,0},{6,2},{1,5},{3,7},{5,1},{7,3},{8,12},{10,14},{12... | collective-permute-start | bytes 1419272 | tf_op jit(solution)/shard_map/ppermute | solution.py:350
  90.4 13.6 %collective-permute-start.4 = (bf16[2,2,1408]{2,1,0:T(2,128)(2,1)S(1)}, bf16[2,2,1408]{2,1,0:T(2,128)(2,1)S(1)}, u32[]{:S(2)}, u32[]{:S(2)}) collective-permute-start(bf16[2,2,1408]{2,1,0:T(2,128)(2,1)S(1)} %pad_maximum_fusion.1), channel_id=1, source_target_pairs={{2,0},{4,2},{6,4},{3,1},{5,3},{7,5},{10,8},{12,10},{14,12},{11,9},... | collective-permute-start | bytes 33800 | tf_op jit(solution)/shard_map/ppermute | solution.py:28
  104.1 0.6 copy-start.13
  104.1 0.8 copy-start.9
  104.1 0.9 copy-start.10
  104.1 1.1 copy-start.11
  110.3 0.8 copy-start.3
